TPU v7x, 32 devices: a whole 2x2x4 slice. The times are simulated.
32 devices in a mesh: grp: 2 (over y), sp: 4 (over z), tp: 4 (over x, core).
Axes of the slice: x: 2, y: 2, z: 4, core: 2. Of those that a mesh axis runs over, the one named last changes fastest.
Arguments:
- queries: bfloat16 [4096, 1024], P(('grp', 'sp'), 'tp'), parts along dimension 0, may hold values from -6 to 6
- memory_keys: bfloat16 [4096, 1024], P(('grp', 'sp'), 'tp'), parts along dimension 0, may hold values from -6 to 6
- memory_values: bfloat16 [4096, 1024], P(('grp', 'sp'), 'tp'), parts along dimension 0, may hold values from -6 to 6
- output_preactivation: bfloat16 [4096, 1024], P(('grp', 'sp'), 'tp'), parts along dimension 0, may hold values from -12 to 12
- input_preactivation: float32 [8, 4096], P('tp', ('grp', 'sp')), parts along dimension 1, may hold values from -6 to 140
- forget_preactivation: float32 [8, 4096], P('tp', ('grp', 'sp')), parts along dimension 1, as said below
- extra_forget_terms: float32 [8, 4096], P('tp', ('grp', 'sp')), parts along dimension 1, may hold values from -1 to 0, as said below
- head_norm_gain: float32 [128], replicated, may hold values from 0.1 to 1.9
- output_projection_matrix: bfloat16 [1024, 2048], P('tp'), may hold values from -0.1875 to 0.1875
- residual: bfloat16 [4096, 2048], P(('grp', 'sp', 'tp')), parts along dimension 0, may hold values from -6 to 6
- feedforward_norm_gain: float32 [2048], replicated, may hold values from 0.1 to 1.9
- feedforward_up_matrix: bfloat16 [2048, 8192], P('sp', 'tp'), may hold values from -0.125 to 0.125
- feedforward_down_matrix: bfloat16 [8192, 2048], P('tp', 'sp'), may hold values from -0.0625 to 0.0625
Outputs:
- layer_out: bfloat16 [4096, 2048], P(('grp', 'sp', 'tp')), parts along dimension 0
There are 2 independent parts, one for each index of `grp`. A program takes and returns all parts, laid end to end along the dimension named above; an argument that names none is the same for every part. Nothing has to cross between parts.
Inputs may be any that keep to these rules, and one draw needn't show every extreme that they name: `forget_preactivation`: forget gate pre-activations. `extra_forget_terms`: extra log forget terms, zero at most positions.
All inputs are finite; a program needn't handle non-finite values.
Results may differ from a plain program's by a relative error of at most 0.018.
Values may be sent and summed in bfloat16 or wider, within the bound.
A program may use at most 64 MiB of HBM per device.

v0:
```python
import functools

import jax
import jax.numpy as jnp
from jax import lax
from jax.experimental import pallas as pl
from jax.experimental.pallas import tpu as pltpu
from jax.sharding import PartitionSpec as P

BLOCK = 128
EPS = 1e-06
NEG = -1e30
MESH = pl.DeviceIdType.MESH
F32 = jnp.float32
BF16 = jnp.bfloat16


def split_dot(exact, wide, swap=False):
    high = wide.astype(BF16)
    low = (wide - high.astype(F32)).astype(BF16)
    if swap:
        return jnp.dot(high, exact, preferred_element_type=F32) + jnp.dot(
            low, exact, preferred_element_type=F32
        )
    return jnp.dot(exact, high, preferred_element_type=F32) + jnp.dot(
        exact, low, preferred_element_type=F32
    )


def kernel(
    dims,
    q_ref, k_ref, v_ref, o_ref, arow_ref, acol_ref, ccol_ref, hgain_ref, wout_ref, res_ref,
    fgain_ref, up_ref, down_ref,
    mid_ref, mlp_ref,
    upw, dnw, ntok, act, psend, precv, msend, mrecv, cbuf, crecv, bsend, brecv, mixed, blockmem, st_out, st_in,
    w_send, w_recv, loc_sem, st_send, st_recv, c_send, c_recv, b_send, b_recv, t_send, t_recv, f_send,
    p_send, p_recv, m_send, m_recv,
):
    grp, sp, tp, heads, blocks, rows = dims
    g, z, t = lax.axis_index("grp"), lax.axis_index("sp"), lax.axis_index("tp")
    layer = grp * tp
    me = g * tp + t
    half = tp // 2
    same = grp * half
    core = lax.rem(t, 2)
    pair = t // 2
    place = g * half + pair
    mine = core * same + place
    partner = t + 1 - 2 * core
    counts = (upw.shape[1], dnw.shape[1])

    def there(gg, zz, tt):
        return {"grp": gg, "sp": zz, "tp": tt}

    barrier = pltpu.get_barrier_semaphore()
    for j in range(1, layer):
        d = lax.rem(me + j, layer)
        pl.semaphore_signal(
            barrier, inc=1, device_id=there(d // tp, z, lax.rem(d, tp)), device_id_type=MESH
        )

    @pl.when(z > 0)
    def _():
        pl.semaphore_signal(barrier, inc=1, device_id=there(g, z - 1, t), device_id_type=MESH)

    @pl.when(z < sp - 1)
    def _():
        pl.semaphore_signal(barrier, inc=1, device_id=there(g, z + 1, t), device_id_type=MESH)

    neighbours = (z + sp - 1) // sp + (2 * sp - 2 - z) // sp
    pl.semaphore_wait(barrier, layer - 1 + neighbours)

    hidden_half = up_ref.shape[1] // grp
    bufs = (upw, dnw)

    def own_piece(m, c):
        n = bufs[m].shape[2]
        if m == 0:
            return up_ref.at[
                pl.ds(c * n, n), pl.ds(pl.multiple_of(g * hidden_half, 128), hidden_half)
            ]
        n = bufs[m].shape[3]
        return down_ref.at[
            pl.ds(pl.multiple_of(g * hidden_half, 16), hidden_half), pl.ds(c * n, n)
        ]

    def weight_copy(m, c, origin, way, source=None):
        dst = bufs[m].at[origin, c]
        zz = z + 1 if way == 0 else z - 1
        return pltpu.make_async_remote_copy(
            src_ref=dst if source is None else source,
            dst_ref=dst,
            send_sem=w_send.at[m, way, origin, c],
            recv_sem=w_recv.at[m, origin, c],
            device_id=there(g, zz, t),
            device_id_type=MESH,
        )

    def local_copy(m, c):
        return pltpu.make_async_copy(own_piece(m, c), bufs[m].at[z, c], loc_sem.at[m, c])

    def start_right(m, c):
        @pl.when(z < sp - 1)
        def _():
            weight_copy(m, c, z, 0, own_piece(m, c)).start()

    def start_left(m, c):
        @pl.when(z > 0)
        def _():
            weight_copy(m, c, z, 1, own_piece(m, c)).start()

    def relay(m, s, c):
        left, right = z - 1 - s, z + 1 + s

        @pl.when(left >= 0)
        def _():
            weight_copy(m, c, left, 0).wait_recv()

            @pl.when(z < sp - 1)
            def _():
                weight_copy(m, c, left, 0).start()

        @pl.when(right < sp)
        def _():
            weight_copy(m, c, right, 1).wait_recv()

            @pl.when(z > 0)
            def _():
                weight_copy(m, c, right, 1).start()

    def relays(first, last):
        def body(s, _):
            for c in range(counts[0]):
                relay(0, s, c)
            return 0

        lax.fori_loop(first, last, body, 0)

    start_right(0, 0)

    @pl.when(z > 1)
    def _():
        for c in range(1, counts[0]):
            start_right(0, c)

    for m in range(2):
        for c in range(counts[m]):
            start_left(m, c)
    for m in range(2):
        for c in range(counts[m]):
            local_copy(m, c).start()

    scale = BLOCK ** (-0.5) if q_ref.shape[1] // heads == BLOCK else (q_ref.shape[1] // heads) ** (-0.5)
    dh = q_ref.shape[1] // heads
    totals, tails = {}, {}
    for h in range(heads):
        cols = pl.ds(h * dh, dh)
        run = None
        for b in range(blocks):
            at = pl.ds(b * BLOCK, BLOCK)
            cum = ccol_ref[at, h : h + 1]
            total = cum[BLOCK - 1 : BLOCK, :]
            tail = total + acol_ref[at, h : h + 1]
            tail_max = jnp.max(tail, axis=0, keepdims=True)
            weighted = v_ref[at, cols].astype(F32) * jnp.exp(tail - tail_max)
            key_t = k_ref[at, cols].astype(F32).T.astype(BF16)
            mem = split_dot(key_t, weighted) * scale
            blockmem[h, b] = mem
            totals[h, b], tails[h, b] = total, tail_max
            if run is None:
                run = (total, tail_max, mem)
            else:
                new = jnp.maximum(total + run[1], tail_max)
                run = (
                    total + run[0],
                    new,
                    jnp.exp(total + run[1] - new) * run[2] + jnp.exp(tail_max - new) * mem,
                )
        st_out[h, :dh, :] = run[2]
        st_out[h, dh : dh + 8, :] = jnp.broadcast_to(run[1], (8, dh))
        st_out[h, dh + 8 : dh + 16, :] = jnp.broadcast_to(run[0], (8, dh))

    def state_copy():
        return pltpu.make_async_remote_copy(
            src_ref=st_out,
            dst_ref=st_in,
            send_sem=st_send,
            recv_sem=st_recv,
            device_id=there(g, z + 1, t),
            device_id_type=MESH,
        )

    @pl.when(z == 0)
    def _():
        st_in[...] = jnp.zeros_like(st_in)

    @pl.when(z > 0)
    def _():
        state_copy().wait_recv()

    @pl.when(z < sp - 1)
    def _():
        for h in range(heads):
            m_in = st_in[h, dh : dh + 1, :]
            m_loc = st_out[h, dh : dh + 1, :]
            total = st_out[h, dh + 8 : dh + 9, :]
            new = jnp.maximum(total + m_in, m_loc)
            st_out[h, :dh, :] = (
                jnp.exp(total + m_in - new) * st_in[h, :dh, :]
                + jnp.exp(m_loc - new) * st_out[h, :dh, :]
            )
            st_out[h, dh : dh + 8, :] = jnp.broadcast_to(new, (8, dh))
        state_copy().start()

    @pl.when(z <= 1)
    def _():
        for c in range(1, counts[0]):
            start_right(0, c)

    for c in range(counts[1]):
        start_right(1, c)

    third = (sp - 1) // 3
    relays(0, third)

    causal = lax.broadcasted_iota(jnp.int32, (BLOCK, BLOCK), 0) >= lax.broadcasted_iota(
        jnp.int32, (BLOCK, BLOCK), 1
    )
    gain = hgain_ref[...]
    for h in range(heads):
        cols = pl.ds(h * dh, dh)
        memory = st_in[h, :dh, :]
        stab = st_in[h, dh : dh + 1, 0:1]
        for b in range(blocks):
            at = pl.ds(b * BLOCK, BLOCK)
            cum = ccol_ref[at, h : h + 1]
            query = q_ref[at, cols]
            key_t = k_ref[at, cols].astype(F32).T.astype(BF16)
            log_weight = jnp.where(causal, cum + arow_ref[h * blocks + b : h * blocks + b + 1, :], NEG)
            carry = cum + stab
            row_max = jnp.maximum(jnp.max(log_weight, axis=1, keepdims=True), carry)
            scores = (
                jnp.dot(query, key_t, preferred_element_type=F32)
                * scale
                * jnp.exp(log_weight - row_max)
            )
            hidden = split_dot(v_ref[at, cols], scores, swap=True)
            hidden = hidden + jnp.exp(carry - row_max) * split_dot(query, memory)
            mean_sq = jnp.mean(hidden * hidden, axis=1, keepdims=True)
            gate = o_ref[at, cols].astype(F32)
            out = hidden * lax.rsqrt(mean_sq + EPS) * gain * (1.0 / (1.0 + jnp.exp(-gate)))
            mixed[at, cols] = out.astype(BF16)
            total, tail_max = totals[h, b], tails[h, b]
            new = jnp.maximum(total + stab, tail_max)
            memory = jnp.exp(total + stab - new) * memory + jnp.exp(tail_max - new) * blockmem[h, b]
            stab = new

    def cross_copy(q):
        return pltpu.make_async_remote_copy(
            src_ref=cbuf.at[q],
            dst_ref=crecv.at[q],
            send_sem=c_send.at[q],
            recv_sem=c_recv.at[q],
            device_id=there(g, z, partner),
            device_id_type=MESH,
        )

    def branch_copy(q, slot):
        return pltpu.make_async_remote_copy(
            src_ref=bsend.at[q],
            dst_ref=brecv.at[slot],
            send_sem=b_send.at[q],
            recv_sem=b_recv.at[slot],
            device_id=there(g, z, 2 * q + core),
            device_id_type=MESH,
        )

    def branch_part(d):
        return jnp.dot(
            mixed[pl.ds(pl.multiple_of(d * rows, rows), rows), :],
            wout_ref[...],
            preferred_element_type=F32,
        )

    for q in range(half):
        cbuf[q] = branch_part(2 * q + 1 - core).astype(BF16)
        cross_copy(q).start()
    for q in range(half):
        part = branch_part(2 * q + core)
        cross_copy(q).wait_recv()
        bsend[q] = (part + crecv[q].astype(F32)).astype(BF16)

        @pl.when(q != pair)
        def _():
            branch_copy(q, pair).start()

    brecv[pair] = bsend[pair]
    branch = res_ref[...].astype(F32)
    for q in range(half):
        @pl.when(q != pair)
        def _():
            branch_copy(q, q).wait_recv()

        branch = branch + brecv[q].astype(F32)
    mid = branch.astype(BF16)
    mid_ref[...] = mid
    wide = mid.astype(F32)
    mean_sq = jnp.mean(wide * wide, axis=1, keepdims=True)
    ntok[mine] = (wide * lax.rsqrt(mean_sq + EPS) * fgain_ref[...]).astype(BF16)

    def token_copy(j, slot):
        at = lax.rem(place + j, same)
        return pltpu.make_async_remote_copy(
            src_ref=ntok.at[slot],
            dst_ref=ntok.at[slot],
            send_sem=t_send.at[j],
            recv_sem=t_recv.at[slot],
            device_id=there(at // half, z, lax.rem(at, half) * 2 + core),
            device_id_type=MESH,
        )

    def partner_copy(j, side):
        slot = side * same + lax.rem(place + j, same)
        return pltpu.make_async_remote_copy(
            src_ref=ntok.at[slot],
            dst_ref=ntok.at[slot],
            send_sem=f_send.at[j],
            recv_sem=t_recv.at[slot],
            device_id=there(g, z, partner),
            device_id_type=MESH,
        )

    for j in range(1, same):
        token_copy(j, mine).start()
    partner_copy(0, core).start()
    relays(third, 2 * third)
    for c in range(counts[0]):
        local_copy(0, c).wait()

    width = ntok.shape[2]

    def up_half(side):
        def up_step(i, _):
            at = pl.ds(side * same + i * 2, 2)
            x = ntok[at].reshape(2 * rows, width)
            y = jnp.dot(x, upw[...].reshape(width, hidden_half), preferred_element_type=F32)
            y = jnp.maximum(y, 0.0)
            act[at] = (y * y).astype(BF16).reshape(2, rows, hidden_half)
            return 0

        lax.fori_loop(0, same // 2, up_step, 0)

    for j in range(1, same):
        token_copy(j, core * same + lax.rem(place + j, same)).wait_recv()
        partner_copy(j, core).start()
    relays(2 * third, sp - 1)
    for c in range(counts[1]):
        relay(1, 0, c)
    up_half(core)
    for j in range(same):
        partner_copy(j, 1 - core).wait_recv()
    up_half(1 - core)
    for c in range(counts[1]):
        local_copy(1, c).wait()

    pieces = counts[1]

    def pre_copy(unit):
        return pltpu.make_async_remote_copy(
            src_ref=psend.at[unit],
            dst_ref=precv.at[unit],
            send_sem=p_send.at[unit],
            recv_sem=p_recv.at[unit],
            device_id=there(g, z, partner),
            device_id_type=MESH,
        )

    def mlp_copy(unit, p, slot):
        return pltpu.make_async_remote_copy(
            src_ref=msend.at[unit, p],
            dst_ref=mrecv.at[unit, slot],
            send_sem=m_send.at[unit, p],
            recv_sem=m_recv.at[unit, slot],
            device_id=there(p // half, z, 2 * (p % half) + core),
            device_id_type=MESH,
        )

    def down_piece(origin, c):
        unit = origin * pieces + c

        def product(side):
            x = act[pl.ds(side * same, same)].reshape(same * rows, hidden_half)
            return jnp.dot(x, dnw[origin, c], preferred_element_type=F32)

        psend[unit] = product(1 - core).astype(BF16).reshape(psend.shape[1:])
        pre_copy(unit).start()
        own = product(core).reshape(psend.shape[1:])
        pre_copy(unit).wait_recv()
        msend[unit] = (own + precv[unit].astype(F32)).astype(BF16)
        for p in range(same):
            @pl.when(p != place)
            def _():
                mlp_copy(unit, p, place).start()

    for c in range(pieces):
        down_piece(z, c)

    def down_step(s, _):
        for c in range(pieces):
            @pl.when(s > 0)
            def _():
                relay(1, s, c)

            @pl.when(z - 1 - s >= 0)
            def _():
                down_piece(z - 1 - s, c)

            @pl.when(z + 1 + s < sp)
            def _():
                down_piece(z + 1 + s, c)

        return 0

    lax.fori_loop(0, sp - 1, down_step, 0)

    def finish_unit(origin, c):
        unit = origin * pieces + c
        mrecv[unit, place] = msend[unit, place]
        total = jnp.zeros(mrecv.shape[2:], F32)
        for p in range(same):
            @pl.when(p != place)
            def _():
                mlp_copy(unit, p, p).wait_recv()

            total = total + mrecv[unit, p].astype(F32)
        n = mrecv.shape[3]
        mlp_ref[origin, :, c * n : (c + 1) * n] = total

    def finish_pair(s, _):
        @pl.when(z - s >= 0)
        def _():
            for c in range(pieces):
                finish_unit(z - s, c)

        @pl.when((s > 0) & (z + s < sp))
        def _():
            for c in range(pieces):
                finish_unit(z + s, c)

        return 0

    lax.fori_loop(0, sp, finish_pair, 0)

    def drain(origin, _):
        for c in range(pieces):
            unit = origin * pieces + c
            pre_copy(unit).wait_send()
            for p in range(same):
                @pl.when(p != place)
                def _():
                    mlp_copy(unit, p, place).wait_send()
        for m in range(2):
            for c in range(counts[m]):
                @pl.when((origin <= z) & (z < sp - 1))
                def _():
                    weight_copy(m, c, origin, 0).wait_send()

                @pl.when((origin >= z) & (z > 0))
                def _():
                    weight_copy(m, c, origin, 1).wait_send()
        return 0

    lax.fori_loop(0, sp, drain, 0)
    for q in range(half):
        cross_copy(q).wait_send()

        @pl.when(q != pair)
        def _():
            branch_copy(q, pair).wait_send()

    for j in range(1, same):
        token_copy(j, mine).wait_send()
    for j in range(same):
        partner_copy(j, core).wait_send()

    @pl.when(z < sp - 1)
    def _():
        state_copy().wait_send()


def shards(
    mesh_shape,
    queries, memory_keys, memory_values, output_preactivation, input_preactivation,
    forget_preactivation, extra_forget_terms, head_norm_gain, output_projection_matrix, residual,
    feedforward_norm_gain, feedforward_up_matrix, feedforward_down_matrix,
):
    grp, sp, tp = mesh_shape
    tokens = queries.shape[0]
    heads = input_preactivation.shape[0]
    blocks = tokens // BLOCK
    dh = queries.shape[1] // heads
    rows, width = residual.shape
    layer = grp * tp
    up_rows, hidden = feedforward_up_matrix.shape
    hidden_half = hidden // grp
    out_cols = feedforward_down_matrix.shape[1]
    chunks = 2
    pieces = 2 if out_cols % 256 == 0 else 1
    half = tp // 2
    same = grp * half
    units = sp * pieces

    log_forget = jax.nn.log_sigmoid(forget_preactivation) + extra_forget_terms
    cum = jnp.cumsum(log_forget.reshape(heads, blocks, BLOCK), axis=-1)
    rest = input_preactivation.reshape(heads, blocks, BLOCK) - cum
    arow = rest.reshape(heads * blocks, BLOCK)
    acol = rest.reshape(heads, tokens).T
    ccol = cum.reshape(heads, tokens).T

    vmem = pl.BlockSpec(memory_space=pltpu.VMEM)
    hbm = pl.BlockSpec(memory_space=pl.ANY)
    dma = pltpu.SemaphoreType.DMA
    mid, mlp = pl.pallas_call(
        functools.partial(kernel, (grp, sp, tp, heads, blocks, rows)),
        out_shape=(
            jax.ShapeDtypeStruct((rows, width), BF16),
            jax.ShapeDtypeStruct((sp, rows, out_cols), F32),
        ),
        in_specs=[vmem] * 11 + [hbm] * 2,
        out_specs=(vmem, vmem),
        scratch_shapes=[
            pltpu.VMEM((sp, chunks, up_rows // chunks, hidden_half), BF16),
            pltpu.VMEM((sp, pieces, hidden_half, out_cols // pieces), BF16),
            pltpu.VMEM((layer, rows, width), BF16),
            pltpu.VMEM((layer, rows, hidden_half), BF16),
            pltpu.VMEM((units, same, rows, out_cols // pieces), BF16),
            pltpu.VMEM((units, same, rows, out_cols // pieces), BF16),
            pltpu.VMEM((units, same, rows, out_cols // pieces), BF16),
            pltpu.VMEM((units, same, rows, out_cols // pieces), BF16),
            pltpu.VMEM((half, rows, width), BF16),
            pltpu.VMEM((half, rows, width), BF16),
            pltpu.VMEM((half, rows, width), BF16),
            pltpu.VMEM((half, rows, width), BF16),
            pltpu.VMEM((tokens, heads * dh), BF16),
            pltpu.VMEM((heads, blocks, dh, dh), F32),
            pltpu.VMEM((heads, dh + 16, dh), F32),
            pltpu.VMEM((heads, dh + 16, dh), F32),
            dma((2, 2, sp, chunks)),
            dma((2, sp, chunks)),
            dma((2, chunks)),
            dma,
            dma,
            dma((half,)),
            dma((half,)),
            dma((half,)),
            dma((half,)),
            dma((same,)),
            dma((layer,)),
            dma((same,)),
            dma((units,)),
            dma((units,)),
            dma((units, same)),
            dma((units, same)),
        ],
        compiler_params=pltpu.CompilerParams(
            collective_id=0, has_side_effects=True, vmem_limit_bytes=60 * 1024 * 1024
        ),
    )(
        queries, memory_keys, memory_values, output_preactivation, arow, acol, ccol,
        head_norm_gain.reshape(1, dh), output_projection_matrix, residual,
        feedforward_norm_gain.reshape(1, width), feedforward_up_matrix, feedforward_down_matrix,
    )
    mlp = mlp.transpose(1, 0, 2).reshape(rows, width)
    return (mid.astype(F32) + mlp).astype(BF16)


def solution(mesh):
    in_specs = (
        P(("grp", "sp"), "tp"),
        P(("grp", "sp"), "tp"),
        P(("grp", "sp"), "tp"),
        P(("grp", "sp"), "tp"),
        P("tp", ("grp", "sp")),
        P("tp", ("grp", "sp")),
        P("tp", ("grp", "sp")),
        P(),
        P("tp", None),
        P(("grp", "sp", "tp"), None),
        P(),
        P("sp", "tp"),
        P("tp", "sp"),
    )
    out_specs = P(("grp", "sp", "tp"), None)
    shape = (mesh.shape["grp"], mesh.shape["sp"], mesh.shape["tp"])
    return jax.shard_map(
        functools.partial(shards, shape),
        mesh=mesh,
        in_specs=in_specs,
        out_specs=out_specs,
        check_vma=False,
    )
```

profile of v0, /device:TPU:25, one launch (start us, length us, event | category | flops | bytes accessed | tf_op | source)
XLA Modules:
  0.0 160.5 jit_solution(13003138478368743041)
XLA Ops:
  0.0 0.7 fusion.1
  0.7 0.6 reduce_window_sum.15
  1.4 0.7 reshape.21
  2.1 0.6 sub.7.arow_ref
  2.7 0.1 copy.16
  2.8 0.0 copy-start
  2.8 0.9 copy.17
  3.7 0.7 bitcast_subtract_fusion
  4.4 0.0 copy-done
  4.4 153.2 %shard_map.127 = (bf16[128,2048]{1,0:T(8,128)(2,1)}, f32[4,128,512]{2,1,0:T(8,128)}) custom-call(bf16[512,256]{1,0:T(8,128)(2,1)} %q_ref.1, bf16[512,256]{1,0:T(8,128)(2,1)} %k_ref.1, bf16[512,256]{1,0:T(8,128)(2,1)} %v_ref.1, bf16[512,256]{1,0:T(8,128)(2,1)} %o_ref.1, f32[8,128]{1,0:T(8,128)} %sub.7.arow_ref, f32[512,2]{1,0:T(8,128)} %bitcast.12, ...), custom_call_target="tpu_custom_call" | custom-call | tf_op jit(solution)/shard_map/pallas_call | solution.py:523
  157.6 0.0 copy-start.1
  157.6 1.6 %copy.18 = f32[128,4,512]{0,2,1:T(8,128)S(1)} copy(f32[128,4,512]{2,0,1:T(8,128)} %bitcast.13) | data formatting | bytes 2097152 | tf_op jit(solution)/shard_map/transpose | solution.py:573
  159.2 0.3 copy.19
  159.6 0.0 copy-done.1
  159.6 0.9 add_convert_fusion
  (1 shorter events, 0.0 us)
Async XLA Ops:
  2.8 1.6 %copy-start = (f32[2,4,128]{0,2,1:T(8,128)}, f32[2,4,128]{0,2,1:T(8,128)S(1)}, u32[]{:S(2)}) copy-start(f32[2,4,128]{0,2,1:T(8,128)S(1)} %copy.16) | copy-start | bytes 12292
  157.6 2.0 %copy-start.1 = (bf16[128,2048]{1,0:T(8,128)(2,1)S(1)}, bf16[128,2048]{1,0:T(8,128)(2,1)}, u32[]{:S(2)}) copy-start(bf16[128,2048]{1,0:T(8,128)(2,1)} %get-tuple-element.7) | copy-start | bytes 1572868
where the time goes:
time: 161 us; the launch traced here: 160 us
  Pallas kernels  153 us (95%)
  local copies, waits for them, and re-layouts  3.65 us (2%)
  other arithmetic  3.57 us (2%)
    pallas_call x1, Pallas kernels, shards(): pl.pallas_call(functools.partial(kernel, (grp, sp, tp, heads, blocks, row...  153 us

commit v1 on v0

v1 whole, which is shorter than its diff:
```python
import functools

import jax
import jax.numpy as jnp
from jax import lax
from jax.experimental import pallas as pl
from jax.experimental.pallas import tpu as pltpu
from jax.sharding import PartitionSpec as P

BLOCK = 128
EPS = 1e-06
NEG = -1e30
MESH = pl.DeviceIdType.MESH
F32 = jnp.float32
BF16 = jnp.bfloat16


def split_dot(exact, wide, swap=False):
    high = wide.astype(BF16)
    low = (wide - high.astype(F32)).astype(BF16)
    if swap:
        return jnp.dot(high, exact, preferred_element_type=F32) + jnp.dot(
            low, exact, preferred_element_type=F32
        )
    return jnp.dot(exact, high, preferred_element_type=F32) + jnp.dot(
        exact, low, preferred_element_type=F32
    )


def aligned(start, multiple):
    return start if isinstance(start, int) else pl.multiple_of(start, multiple)


def kernel(
    dims,
    q_hbm, k_hbm, v_hbm, o_hbm, igate_ref, fgate_ref, extra_ref, hgain_ref, wout_hbm, res_hbm,
    fgain_ref, up_hbm, down_hbm,
    out_ref,
    qb, kb, vb, ob, resb, upw, dnw, wo, mixed, mixin, mid, ntok, act, psend, precv, msend, xrecv, zsend, zrecv,
    own_acc, mlp, keyt, memp, hloc, gates, cols_ref, st_out, st_in,
    in_sem, loc_sem, wu_send, wu_recv, wuy_send, wd_send, wd_recv, wdy_send, wo_send, wo_recv, wop_send,
    st_send, st_recv, mx_send, mx_recv, t_recv, tz_send, tx_send, tr_send, f_send,
    p_send, p_recv, x_send, x_recv, z_send, z_recv,
):
    grp, sp, tp, heads, blocks, rows, group, usubs, dsubs, pieces = dims
    g, z, t = lax.axis_index("grp"), lax.axis_index("sp"), lax.axis_index("tp")
    half = tp // 2
    core, x = lax.rem(t, 2), t // 2
    partner = t + 1 - 2 * core
    zi = lax.rem(z, group)
    other = z + 1 - 2 * zi
    same = half * group
    place = x * group + zi
    mine = core * same + place
    width = ntok.shape[2]
    part = upw.shape[2]
    up_rows = upw.shape[1]
    out_cols = dnw.shape[2]
    n = out_cols // pieces
    urows = up_rows // grp // usubs
    drows = part // grp // dsubs

    def there(gg, zz, tt):
        return {"grp": gg, "sp": zz, "tp": tt}

    def remote(src, dst, send, recv, where):
        return pltpu.make_async_remote_copy(
            src_ref=src, dst_ref=dst, send_sem=send, recv_sem=recv, device_id=where, device_id_type=MESH
        )

    def nth(k):
        power = sp & (sp - 1) == 0
        if not power:
            return lax.rem(z + k, sp)
        gray_of = k
        total = 0
        bit = 1
        while bit < sp:
            mask = (gray_of // bit + gray_of // (2 * bit)) % 2
            zbit = lax.rem(z // bit, 2)
            total = total + (zbit + mask - 2 * zbit * mask) * bit
            bit *= 2
        return total

    def load(i, src, dst):
        return pltpu.make_async_copy(src, dst, in_sem.at[i])

    loads = [load(i, s, d) for i, (s, d) in enumerate(
        ((k_hbm, kb), (v_hbm, vb), (q_hbm, qb), (o_hbm, ob), (res_hbm, resb))
    )]
    for c in loads:
        c.start()

    barrier = pltpu.get_barrier_semaphore()
    for j in range(1, tp):
        pl.semaphore_signal(barrier, inc=1, device_id=there(g, z, lax.rem(t + j, tp)), device_id_type=MESH)
    for j in range(1, grp):
        pl.semaphore_signal(barrier, inc=1, device_id=there(lax.rem(g + j, grp), z, t), device_id_type=MESH)

    def greet(j, _):
        pl.semaphore_signal(barrier, inc=1, device_id=there(g, lax.rem(z + j, sp), t), device_id_type=MESH)
        return 0

    lax.fori_loop(1, sp, greet, 0)
    pl.semaphore_wait(barrier, tp + grp + sp - 3)

    def up_rows_of(c, s):
        return pl.ds(aligned(c * (urows * usubs) + s * urows, 16), urows)

    def down_rows_of(c, s):
        return pl.ds(aligned(c * (drows * dsubs) + s * drows, 16), drows)

    def up_copy(zz, s):
        return remote(
            up_hbm.at[up_rows_of(g, s), pl.ds(aligned(lax.rem(zz, group) * part, 128), part)],
            upw.at[z, up_rows_of(g, s), :],
            wu_send.at[zz, s], wu_recv.at[z, g, s], there(g, zz, t),
        )

    def down_copy(zz, s):
        first = lax.rem(zz, group) * part + g * (drows * dsubs) + s * drows
        return remote(
            down_hbm.at[pl.ds(aligned(first, 16), drows), :],
            dnw.at[z, down_rows_of(g, s), :],
            wd_send.at[zz, s], wd_recv.at[z, g, s], there(g, zz, t),
        )

    def up_pass(o, s, j):
        at = upw.at[o, up_rows_of(g, s), :]
        return remote(at, at, wuy_send.at[o, s, j], wu_recv.at[o, g, s], there(lax.rem(g + j, grp), z, t))

    def down_pass(o, s, j):
        at = dnw.at[o, down_rows_of(g, s), :]
        return remote(at, at, wdy_send.at[o, s, j], wd_recv.at[o, g, s], there(lax.rem(g + j, grp), z, t))

    def up_arrived(o, c, s):
        at = upw.at[o, up_rows_of(c, s), :]
        return remote(at, at, wuy_send.at[o, s, 0], wu_recv.at[o, c, s], there(g, z, t))

    def down_arrived(o, c, s):
        at = dnw.at[o, down_rows_of(c, s), :]
        return remote(at, at, wdy_send.at[o, s, 0], wd_recv.at[o, c, s], there(g, z, t))

    def relay_up(k):
        o = nth(k)
        for s in range(usubs):
            up_arrived(o, g, s).wait_recv()
            for j in range(1, grp):
                up_pass(o, s, j).start()

    def relay_down(k):
        o = nth(k)
        for s in range(dsubs):
            down_arrived(o, g, s).wait_recv()
            for j in range(1, grp):
                down_pass(o, s, j).start()

    def finish_up(k):
        o = nth(k)
        for s in range(usubs):
            for j in range(1, grp):
                up_arrived(o, lax.rem(g + j, grp), s).wait_recv()

    def finish_down(k):
        o = nth(k)
        for s in range(dsubs):
            for j in range(1, grp):
                down_arrived(o, lax.rem(g + j, grp), s).wait_recv()

    def right(copy, first, last, subs, when=True):
        def body(d, _):
            @pl.when((z + d < sp) & when)
            def _():
                for s in subs:
                    copy(z + d, s).start()

            return 0

        lax.fori_loop(first, last, body, 0)

    def left(copy, first, last, subs, when=True):
        def body(d, _):
            @pl.when((z - d >= 0) & when)
            def _():
                for s in subs:
                    copy(z - d, s).start()

            return 0

        lax.fori_loop(first, last, body, 0)

    us, ds = range(usubs), range(dsubs)
    held_right, held_left = zi == 0, zi == group - 1
    right(up_copy, 1, 2, us[:1])
    left(up_copy, 1, sp, us)
    left(down_copy, 1, sp, ds, zi != group - 1)
    left(down_copy, 1, 2, ds[: dsubs // 2], held_left)

    def wo_copy(tt):
        return remote(wout_hbm, wo.at[t], wo_send.at[tt], wo_recv.at[t], there(g, z, tt))

    def wo_pass(j):
        tt = lax.rem(x + j, half) * 2 + core
        return remote(wo.at[tt], wo.at[tt], wop_send.at[j], wo_recv.at[tt], there(g, z, partner))

    def wo_arrived(tt):
        return remote(wo.at[tt], wo.at[tt], wop_send.at[0], wo_recv.at[tt], there(g, z, partner))

    for j in range(1, half):
        wo_copy(lax.rem(x + j, half) * 2 + core).start()
    wo_copy(partner).start()
    own = [
        pltpu.make_async_copy(wout_hbm, wo.at[t], loc_sem.at[0]),
        pltpu.make_async_copy(up_hbm.at[:, pl.ds(aligned(zi * part, 128), part)], upw.at[z], loc_sem.at[1]),
        pltpu.make_async_copy(down_hbm.at[pl.ds(aligned(zi * part, 16), part), :], dnw.at[z], loc_sem.at[2]),
    ]
    for c in own:
        c.start()

    dh = qb.shape[1] // heads
    scale = dh ** (-0.5)
    count = heads * blocks
    pad = -count % 8

    def stacked(value):
        pieces_of = [
            value[h : h + 1, b * BLOCK : (b + 1) * BLOCK] for h in range(heads) for b in range(blocks)
        ]
        if pad:
            pieces_of.append(jnp.zeros((pad, BLOCK), F32))
        return jnp.concatenate(pieces_of, axis=0)

    pre = fgate_ref[...]
    log_forget = jnp.minimum(pre, 0.0) - jnp.log1p(jnp.exp(-jnp.abs(pre))) + extra_ref[...]
    cum_row = stacked(log_forget)
    lane = lax.broadcasted_iota(jnp.int32, cum_row.shape, 1)
    step = 1
    while step < BLOCK:
        cum_row = cum_row + jnp.where(lane >= step, pltpu.roll(cum_row, step, 1), 0.0)
        step *= 2
    rest_row = stacked(igate_ref[...]) - cum_row
    cum_col = cum_row.T
    rest_col = rest_row.T

    loads[0].wait()
    loads[1].wait()
    before, totals = {}, {}
    for h in range(heads):
        cols = pl.ds(h * dh, dh)
        run = None
        for b in range(blocks):
            i = h * blocks + b
            at = pl.ds(b * BLOCK, BLOCK)
            total = cum_row[i : i + 1, BLOCK - 1 : BLOCK]
            tail = total + rest_col[:, i : i + 1]
            tail_max = jnp.max(tail, axis=0, keepdims=True)
            weighted = vb[at, cols].astype(F32) * jnp.exp(tail - tail_max)
            key_t = kb[at, cols].astype(F32).T.astype(BF16)
            keyt[h, b] = key_t
            mem = split_dot(key_t, weighted) * scale
            if run is None:
                run = (total, tail_max, mem)
            else:
                before[h, b] = (run[0], run[1])
                memp[h, b] = run[2]
                new = jnp.maximum(total + run[1], tail_max)
                run = (
                    total + run[0],
                    new,
                    jnp.exp(total + run[1] - new) * run[2] + jnp.exp(tail_max - new) * mem,
                )
        st_out[h, :dh, :] = run[2]
        st_out[h, dh : dh + 8, :] = jnp.broadcast_to(run[1], (8, dh))
        st_out[h, dh + 8 : dh + 16, :] = jnp.broadcast_to(run[0], (8, dh))

    def state_copy():
        return remote(st_out, st_in, st_send, st_recv, there(g, z + 1, t))

    @pl.when(z == 0)
    def _():
        st_in[...] = jnp.zeros_like(st_in)

    def state_on():
        for h in range(heads):
            m_in = st_in[h, dh : dh + 1, :]
            m_loc = st_out[h, dh : dh + 1, :]
            total = st_out[h, dh + 8 : dh + 9, :]
            new = jnp.maximum(total + m_in, m_loc)
            st_out[h, :dh, :] = (
                jnp.exp(total + m_in - new) * st_in[h, :dh, :] + jnp.exp(m_loc - new) * st_out[h, :dh, :]
            )
            st_out[h, dh : dh + 8, :] = jnp.broadcast_to(new, (8, dh))
        state_copy().start()

    def rest_of_sends():
        right(up_copy, 1, 2, us[1:], z == 0)
        right(up_copy, 2, sp, us)
        right(down_copy, 1, sp, ds, zi != 0)

    right(up_copy, 1, 2, us[1:], z > 0)

    @pl.when((z == 0) & (sp > 1))
    def _():
        state_on()

    @pl.when(z == 0)
    def _():
        rest_of_sends()

    loads[2].wait()
    loads[3].wait()
    causal = lax.broadcasted_iota(jnp.int32, (BLOCK, BLOCK), 0) >= lax.broadcasted_iota(
        jnp.int32, (BLOCK, BLOCK), 1
    )
    gain = hgain_ref[...]

    def take_state(when):
        @pl.when(when)
        def _():
            state_copy().wait_recv()

            @pl.when(z < sp - 1)
            def _():
                state_on()

            rest_of_sends()

    for h in range(heads):
        cols = pl.ds(h * dh, dh)
        if h == heads - 1:
            take_state(z == 1)
        for b in range(blocks):
            i = h * blocks + b
            at = pl.ds(b * BLOCK, BLOCK)
            cum = cum_col[:, i : i + 1]
            query = qb[at, cols]
            log_weight = jnp.where(causal, cum + rest_row[i : i + 1, :], NEG)
            row_max = jnp.max(log_weight, axis=1, keepdims=True)
            base = cum
            if b > 0:
                past, stab = before[h, b]
                base = cum + past
                carry = cum + stab
                row_max = jnp.maximum(row_max, carry)
            scores = (
                jnp.dot(query, keyt[h, b], preferred_element_type=F32)
                * scale
                * jnp.exp(log_weight - row_max)
            )
            hidden = split_dot(vb[at, cols], scores, swap=True)
            if b > 0:
                hidden = hidden + jnp.exp(carry - row_max) * split_dot(query, memp[h, b])
            hloc[at, cols] = hidden
            cols_ref[at, 2 * h : 2 * h + 1] = row_max
            cols_ref[at, 2 * h + 1 : 2 * h + 2] = base
            gates[at, cols] = gain * (1.0 / (1.0 + jnp.exp(-ob[at, cols].astype(F32))))

    take_state(z > 1)
    if sp > 1:
        relay_up(1)
    for j in range(1, half):
        wo_arrived(lax.rem(x + j, half) * 2 + core).wait_recv()
        wo_pass(j).start()

    for h in range(heads):
        cols = pl.ds(h * dh, dh)
        memory = st_in[h, :dh, :]
        stab = st_in[h, dh : dh + 1, 0:1]
        for b in range(blocks):
            at = pl.ds(b * BLOCK, BLOCK)
            local_max = cols_ref[at, 2 * h : 2 * h + 1]
            carry = cols_ref[at, 2 * h + 1 : 2 * h + 2] + stab
            row_max = jnp.maximum(local_max, carry)
            hidden = jnp.exp(local_max - row_max) * hloc[at, cols] + jnp.exp(carry - row_max) * split_dot(
                qb[at, cols], memory
            )
            mean_sq = jnp.mean(hidden * hidden, axis=1, keepdims=True)
            mixed[at, cols] = (hidden * lax.rsqrt(mean_sq + EPS) * gates[at, cols]).astype(BF16)

    def mixed_copy(j):
        d = lax.rem(t + j, tp)
        return remote(
            mixed.at[pl.ds(aligned(d * rows, 16), rows), :],
            mixin.at[t], mx_send.at[j], mx_recv.at[t], there(g, z, d),
        )

    def mixed_arrived(tt):
        return remote(mixin.at[tt], mixin.at[tt], mx_send.at[0], mx_recv.at[tt], there(g, z, partner))

    for j in range(1, tp):
        mixed_copy(j).start()
    mixin[t] = mixed[pl.ds(aligned(t * rows, 16), rows), :]
    own[0].wait()
    loads[4].wait()
    for j in range(1, half):
        wo_arrived(lax.rem(x + j, half) * 2 + 1 - core).wait_recv()
    wo_arrived(partner).wait_recv()
    for j in range(1, tp):
        mixed_arrived(lax.rem(t + j, tp)).wait_recv()

    chunk = min(512, width)
    sum_sq = jnp.zeros((rows, 1), F32)
    for c in range(width // chunk):
        at = pl.ds(c * chunk, chunk)
        branch = jnp.zeros((rows, chunk), F32)
        for tt in range(tp):
            branch = branch + jnp.dot(mixin[tt], wo[tt, :, at], preferred_element_type=F32).astype(
                BF16
            ).astype(F32)
        value = (resb[:, at].astype(F32) + branch).astype(BF16)
        mid[:, at] = value
        wide = value.astype(F32)
        sum_sq = sum_sq + jnp.sum(wide * wide, axis=1, keepdims=True)
    factor = lax.rsqrt(sum_sq * (1.0 / width) + EPS)
    for c in range(width // chunk):
        at = pl.ds(c * chunk, chunk)
        ntok[mine, :, at] = (mid[:, at].astype(F32) * factor * fgain_ref[:, at]).astype(BF16)

    def slot_of(xx, zz):
        return core * same + xx * group + zz

    def token(slot, send, where):
        return remote(ntok.at[slot], ntok.at[slot], send, t_recv.at[slot], where)

    def to_pair():
        return token(mine, tz_send, there(g, other, t))

    def to_x(j):
        return token(mine, tx_send.at[j], there(g, z, lax.rem(x + j, half) * 2 + core))

    def pass_x(j):
        return token(slot_of(x, 1 - zi), tr_send.at[j], there(g, z, lax.rem(x + j, half) * 2 + core))

    def to_partner(xx, zz):
        slot = slot_of(xx, zz)
        return token(slot, f_send.at[xx * group + zz], there(g, z, partner))

    def arrived(slot):
        return token(slot, tz_send, there(g, z, partner))

    if group > 1:
        to_pair().start()
    for j in range(1, half):
        to_x(j).start()
    to_partner(x, zi).start()
    left(down_copy, 1, 2, ds[dsubs // 2 :], held_left)
    left(down_copy, 2, sp, ds, held_left)
    right(down_copy, 1, sp, ds, held_right)

    def relays_up(first, last):
        def body(k, _):
            relay_up(k)
            return 0

        lax.fori_loop(first, last, body, 0)

    middle = 2 + (sp - 2) // 2
    relays_up(2, middle)
    for j in range(1, half):
        xx = lax.rem(x + j, half)
        arrived(slot_of(xx, zi)).wait_recv()
        to_partner(xx, zi).start()
    if group > 1:
        arrived(slot_of(x, 1 - zi)).wait_recv()
        for j in range(1, half):
            pass_x(j).start()
        to_partner(x, 1 - zi).start()
    relays_up(middle, sp)
    own[1].wait()

    def all_up(k, _):
        finish_up(k)
        return 0

    lax.fori_loop(1, sp, all_up, 0)
    if group > 1:
        for j in range(1, half):
            xx = lax.rem(x + j, half)
            arrived(slot_of(xx, 1 - zi)).wait_recv()
            to_partner(xx, 1 - zi).start()

    def up_half(side):
        def up_step(i, _):
            at = pl.ds(side * same + i * 2, 2)
            value = ntok[at].reshape(2 * rows, width)
            y = jnp.dot(value, upw[...].reshape(width, part), preferred_element_type=F32)
            y = jnp.maximum(y, 0.0)
            act[at] = (y * y).astype(BF16).reshape(2, rows, part)
            return 0

        lax.fori_loop(0, same // 2, up_step, 0)

    up_half(core)
    for xx in range(half):
        for zz in range(group):
            arrived((1 - core) * same + xx * group + zz).wait_recv()
    up_half(1 - core)
    own[2].wait()

    def pre_copy(unit):
        return remote(
            psend.at[unit], precv.at[unit], p_send.at[unit], p_recv.at[unit], there(g, z, partner)
        )

    def x_copy(unit, j):
        xx = lax.rem(x + j, half)
        return remote(
            msend.at[unit, pl.ds(xx * group, group)], xrecv.at[unit, x],
            x_send.at[unit, j], x_recv.at[unit, x], there(g, z, xx * 2 + core),
        )

    def x_arrived(unit, xx):
        at = xrecv.at[unit, xx]
        return remote(at, at, x_send.at[unit, 0], x_recv.at[unit, xx], there(g, z, partner))

    def z_copy(unit):
        return remote(zsend.at[unit], zrecv.at[unit], z_send.at[unit], z_recv.at[unit], there(g, other, t))

    def multiply(m, c):
        k, parity = m // pieces, lax.rem(m, 2)
        o = nth(k)
        unit = o * pieces + c

        def product(side):
            value = act[pl.ds(side * same, same)].reshape(same * rows, part)
            return jnp.dot(value, dnw[o, :, c * n : (c + 1) * n], preferred_element_type=F32)

        psend[unit] = product(1 - core).astype(BF16).reshape(psend.shape[1:])
        pre_copy(unit).start()
        own_acc[parity] = product(core).reshape(psend.shape[1:])

    def unit_of(m):
        return nth(m // pieces) * pieces + lax.rem(m, pieces)

    def spread(m):
        unit = unit_of(m)
        pre_copy(unit).wait_recv()
        msend[unit] = (own_acc[lax.rem(m, 2)] + precv[unit].astype(F32)).astype(BF16)
        for j in range(1, half):
            x_copy(unit, j).start()
        xrecv[unit, x] = msend[unit, pl.ds(x * group, group)]

    def gathered(unit, zz):
        total = xrecv[unit, 0, zz].astype(F32)
        for xx in range(1, half):
            total = total + xrecv[unit, xx, zz].astype(F32)
        return total

    def hand_over(m):
        unit = unit_of(m)
        for j in range(1, half):
            x_arrived(unit, lax.rem(x + j, half)).wait_recv()
        if group > 1:
            zsend[unit] = gathered(unit, 1 - zi).astype(BF16)
            z_copy(unit).start()

    def stage(k, _):
        @pl.when(k > 0)
        def _():
            relay_down(k)
            finish_down(k)

        for c in range(pieces):
            m = k * pieces + c
            multiply(m, c)

            @pl.when(m >= 1)
            def _():
                spread(m - 1)

            @pl.when(m >= 2)
            def _():
                hand_over(m - 2)

        return 0

    lax.fori_loop(0, sp, stage, 0)
    units = sp * pieces
    spread(units - 1)
    if units > 1:
        hand_over(units - 2)
    hand_over(units - 1)

    direct = out_cols % 128 == 0 and n % 128 == 0

    def finish(m, _):
        unit = unit_of(m)
        total = gathered(unit, zi)
        if group > 1:
            z_copy(unit).wait_recv()
            total = total + zrecv[unit].astype(F32)
        if direct:
            at = pl.ds(aligned(unit * n, 128), n)
            out_ref[:, at] = (mid[:, at].astype(F32) + total).astype(BF16)
        else:
            mlp[unit] = total
        return 0

    lax.fori_loop(0, units, finish, 0)
    if not direct:
        for unit in range(units):
            at = pl.ds(unit * n, n)
            out_ref[:, at] = (mid[:, at].astype(F32) + mlp[unit]).astype(BF16)

    def drain(o, _):
        @pl.when(o != z)
        def _():
            for s in us:
                up_copy(o, s).wait_send()
                for j in range(1, grp):
                    up_pass(o, s, j).wait_send()
            for s in ds:
                down_copy(o, s).wait_send()
                for j in range(1, grp):
                    down_pass(o, s, j).wait_send()

        for c in range(pieces):
            unit = o * pieces + c
            pre_copy(unit).wait_send()
            for j in range(1, half):
                x_copy(unit, j).wait_send()
            if group > 1:
                z_copy(unit).wait_send()
        return 0

    lax.fori_loop(0, sp, drain, 0)
    for j in range(1, half):
        wo_copy(lax.rem(x + j, half) * 2 + core).wait_send()
        wo_pass(j).wait_send()
        to_x(j).wait_send()
        if group > 1:
            pass_x(j).wait_send()
    wo_copy(partner).wait_send()
    for j in range(1, tp):
        mixed_copy(j).wait_send()
    if group > 1:
        to_pair().wait_send()
    for xx in range(half):
        for zz in range(group):
            to_partner(xx, zz).wait_send()

    @pl.when(z < sp - 1)
    def _():
        state_copy().wait_send()


def shards(
    mesh_shape,
    queries, memory_keys, memory_values, output_preactivation, input_preactivation,
    forget_preactivation, extra_forget_terms, head_norm_gain, output_projection_matrix, residual,
    feedforward_norm_gain, feedforward_up_matrix, feedforward_down_matrix,
):
    grp, sp, tp = mesh_shape
    tokens, across = queries.shape
    heads = input_preactivation.shape[0]
    blocks = tokens // BLOCK
    dh = across // heads
    rows, width = residual.shape
    up_rows, hidden = feedforward_up_matrix.shape
    out_cols = feedforward_down_matrix.shape[1]
    group = 2 if sp % 2 == 0 else 1
    part = hidden // group
    usubs = 2 if up_rows % (32 * grp) == 0 else 1
    dsubs = 2
    pieces = 2 if out_cols % 256 == 0 else 1
    half = tp // 2
    same = half * group
    layer = tp * group
    units = sp * pieces
    n = out_cols // pieces

    vmem = pl.BlockSpec(memory_space=pltpu.VMEM)
    hbm = pl.BlockSpec(memory_space=pl.ANY)
    dma = pltpu.SemaphoreType.DMA
    return pl.pallas_call(
        functools.partial(
            kernel, (grp, sp, tp, heads, blocks, rows, group, usubs, dsubs, pieces)
        ),
        out_shape=jax.ShapeDtypeStruct((rows, width), BF16),
        in_specs=[hbm] * 4 + [vmem] * 4 + [hbm] * 2 + [vmem] + [hbm] * 2,
        out_specs=vmem,
        scratch_shapes=[
            pltpu.VMEM((tokens, across), BF16),
            pltpu.VMEM((tokens, across), BF16),
            pltpu.VMEM((tokens, across), BF16),
            pltpu.VMEM((tokens, across), BF16),
            pltpu.VMEM((rows, width), BF16),
            pltpu.VMEM((sp, up_rows, part), BF16),
            pltpu.VMEM((sp, part, out_cols), BF16),
            pltpu.VMEM((tp, across, width), BF16),
            pltpu.VMEM((tokens, across), BF16),
            pltpu.VMEM((tp, rows, across), BF16),
            pltpu.VMEM((rows, width), BF16),
            pltpu.VMEM((layer, rows, width), BF16),
            pltpu.VMEM((layer, rows, part), BF16),
            pltpu.VMEM((units, same, rows, n), BF16),
            pltpu.VMEM((units, same, rows, n), BF16),
            pltpu.VMEM((units, same, rows, n), BF16),
            pltpu.VMEM((units, half, group, rows, n), BF16),
            pltpu.VMEM((units, rows, n), BF16),
            pltpu.VMEM((units, rows, n), BF16),
            pltpu.VMEM((2, same, rows, n), F32),
            pltpu.VMEM((units, rows, n) if n % 128 else (1, 8, 128), F32),
            pltpu.VMEM((heads, blocks, dh, BLOCK), BF16),
            pltpu.VMEM((heads, blocks, dh, dh), F32),
            pltpu.VMEM((tokens, across), F32),
            pltpu.VMEM((tokens, across), F32),
            pltpu.VMEM((tokens, 128), F32),
            pltpu.VMEM((heads, dh + 16, dh), F32),
            pltpu.VMEM((heads, dh + 16, dh), F32),
            dma((5,)),
            dma((3,)),
            dma((sp, usubs)),
            dma((sp, grp, usubs)),
            dma((sp, usubs, grp)),
            dma((sp, dsubs)),
            dma((sp, grp, dsubs)),
            dma((sp, dsubs, grp)),
            dma((tp,)),
            dma((tp,)),
            dma((half,)),
            dma,
            dma,
            dma((tp,)),
            dma((tp,)),
            dma((layer,)),
            dma,
            dma((half,)),
            dma((half,)),
            dma((same,)),
            dma((units,)),
            dma((units,)),
            dma((units, half)),
            dma((units, half)),
            dma((units,)),
            dma((units,)),
        ],
        compiler_params=pltpu.CompilerParams(
            collective_id=0, has_side_effects=True, vmem_limit_bytes=60 * 1024 * 1024
        ),
    )(
        queries, memory_keys, memory_values, output_preactivation,
        input_preactivation, forget_preactivation, extra_forget_terms,
        head_norm_gain.reshape(1, dh), output_projection_matrix, residual,
        feedforward_norm_gain.reshape(1, width), feedforward_up_matrix, feedforward_down_matrix,
    )


def solution(mesh):
    in_specs = (
        P(("grp", "sp"), "tp"),
        P(("grp", "sp"), "tp"),
        P(("grp", "sp"), "tp"),
        P(("grp", "sp"), "tp"),
        P("tp", ("grp", "sp")),
        P("tp", ("grp", "sp")),
        P("tp", ("grp", "sp")),
        P(),
        P("tp", None),
        P(("grp", "sp", "tp"), None),
        P(),
        P("sp", "tp"),
        P("tp", "sp"),
    )
    out_specs = P(("grp", "sp", "tp"), None)
    shape = (mesh.shape["grp"], mesh.shape["sp"], mesh.shape["tp"])
    return jax.shard_map(
        functools.partial(shards, shape),
        mesh=mesh,
        in_specs=in_specs,
        out_specs=out_specs,
        check_vma=False,
    )
```

time: 161 us -> 162 us (level)
  the two profiles are of different devices: /device:TPU:25 before, /device:TPU:17 now
where the time goes in v1:
time: 162 us; the launch traced here: 161 us
  Pallas kernels  159 us (98%)
  local copies, waits for them, and re-layouts  1.88 us (1%)
    pallas_call x1, Pallas kernels, shards(): pl.pallas_call(functools.partial(kernel, (grp, sp, tp, heads, blocks, row...  159 us

profile of v1, /device:TPU:17, one launch (start us, length us, event | category | flops | bytes accessed | tf_op | source)
XLA Modules:
  0.0 160.9 jit_solution(14336476909897350892)
XLA Ops:
  0.0 159.0 %shard_map.127 = bf16[128,2048]{1,0:T(8,128)(2,1)} custom-call(bf16[512,256]{1,0:T(8,128)(2,1)} %q_hbm.1, bf16[512,256]{1,0:T(8,128)(2,1)} %k_hbm.1, bf16[512,256]{1,0:T(8,128)(2,1)} %v_hbm.1, bf16[512,256]{1,0:T(8,128)(2,1)} %o_hbm.1, f32[2,512]{1,0:T(2,128)} %igate_ref.1, f32[2,512]{1,0:T(2,128)} %fgate_ref.1, f32[2,512]{1,0:T(2,128)} %extra_ref.1, ...), custom_call_target="tpu_custom_call" | custom-call | tf_op jit(solution)/shard_map/pallas_call | solution.py:675
  159.0 1.9 %copy.15 = bf16[128,2048]{1,0:T(8,128)(2,1)} copy(bf16[128,2048]{1,0:T(8,128)(2,1)} %shard_map.127) | data formatting | bytes 1048576

commit v2 on v1

--- a/solution.py
+++ b/solution.py
@@ -42,7 +42,7 @@
     st_send, st_recv, mx_send, mx_recv, t_recv, tz_send, tx_send, tr_send, f_send,
     p_send, p_recv, x_send, x_recv, z_send, z_recv,
 ):
-    grp, sp, tp, heads, blocks, rows, group, usubs, dsubs, pieces = dims
+    grp, sp, tp, heads, blocks, rows, group, usubs, rsubs, pieces, tsubs = dims
     g, z, t = lax.axis_index("grp"), lax.axis_index("sp"), lax.axis_index("tp")
     half = tp // 2
     core, x = lax.rem(t, 2), t // 2
@@ -50,15 +50,17 @@
     zi = lax.rem(z, group)
     other = z + 1 - 2 * zi
     same = half * group
-    place = x * group + zi
-    mine = core * same + place
+    mine = core * same + zi * half + x
+    edge = (z == 0) | (z == sp - 1)
+    dsubs = rsubs * pieces
     width = ntok.shape[2]
     part = upw.shape[2]
     up_rows = upw.shape[1]
     out_cols = dnw.shape[2]
     n = out_cols // pieces
     urows = up_rows // grp // usubs
-    drows = part // grp // dsubs
+    drows = part // grp // rsubs
+    trows = rows // tsubs
 
     def there(gg, zz, tt):
         return {"grp": gg, "sp": zz, "tp": tt}
@@ -107,8 +109,9 @@
     def up_rows_of(c, s):
         return pl.ds(aligned(c * (urows * usubs) + s * urows, 16), urows)
 
-    def down_rows_of(c, s):
-        return pl.ds(aligned(c * (drows * dsubs) + s * drows, 16), drows)
+    def down_at(c, s):
+        rows_at = pl.ds(aligned(c * (drows * rsubs) + s % rsubs * drows, 16), drows)
+        return rows_at, pl.ds(s // rsubs * n, n)
 
     def up_copy(zz, s):
         return remote(
@@ -118,10 +121,10 @@
         )
 
     def down_copy(zz, s):
-        first = lax.rem(zz, group) * part + g * (drows * dsubs) + s * drows
+        first = lax.rem(zz, group) * part + g * (drows * rsubs) + s % rsubs * drows
         return remote(
-            down_hbm.at[pl.ds(aligned(first, 16), drows), :],
-            dnw.at[z, down_rows_of(g, s), :],
+            down_hbm.at[pl.ds(aligned(first, 16), drows), pl.ds(s // rsubs * n, n)],
+            dnw.at[(z, *down_at(g, s))],
             wd_send.at[zz, s], wd_recv.at[z, g, s], there(g, zz, t),
         )
 
@@ -130,7 +133,7 @@
         return remote(at, at, wuy_send.at[o, s, j], wu_recv.at[o, g, s], there(lax.rem(g + j, grp), z, t))
 
     def down_pass(o, s, j):
-        at = dnw.at[o, down_rows_of(g, s), :]
+        at = dnw.at[(o, *down_at(g, s))]
         return remote(at, at, wdy_send.at[o, s, j], wd_recv.at[o, g, s], there(lax.rem(g + j, grp), z, t))
 
     def up_arrived(o, c, s):
@@ -138,7 +141,7 @@
         return remote(at, at, wuy_send.at[o, s, 0], wu_recv.at[o, c, s], there(g, z, t))
 
     def down_arrived(o, c, s):
-        at = dnw.at[o, down_rows_of(c, s), :]
+        at = dnw.at[(o, *down_at(c, s))]
         return remote(at, at, wdy_send.at[o, s, 0], wd_recv.at[o, c, s], there(g, z, t))
 
     def relay_up(k):
@@ -148,9 +151,12 @@
             for j in range(1, grp):
                 up_pass(o, s, j).start()
 
-    def relay_down(k):
+    def of_piece(c):
+        return range(c * rsubs, (c + 1) * rsubs)
+
+    def relay_down(k, c):
         o = nth(k)
-        for s in range(dsubs):
+        for s in of_piece(c):
             down_arrived(o, g, s).wait_recv()
             for j in range(1, grp):
                 down_pass(o, s, j).start()
@@ -161,14 +167,16 @@
             for j in range(1, grp):
                 up_arrived(o, lax.rem(g + j, grp), s).wait_recv()
 
-    def finish_down(k):
+    def finish_down(k, c):
         o = nth(k)
-        for s in range(dsubs):
+        for s in of_piece(c):
             for j in range(1, grp):
                 down_arrived(o, lax.rem(g + j, grp), s).wait_recv()
 
-    def right(copy, first, last, subs, when=True):
-        def body(d, _):
+    def right(copy, first, last, subs, when=True, flip=False):
+        def body(i, _):
+            d = first + last - 1 - i if flip else i
+
             @pl.when((z + d < sp) & when)
             def _():
                 for s in subs:
@@ -178,8 +186,10 @@
 
         lax.fori_loop(first, last, body, 0)
 
-    def left(copy, first, last, subs, when=True):
-        def body(d, _):
+    def left(copy, first, last, subs, when=True, flip=False):
+        def body(i, _):
+            d = first + last - 1 - i if flip else i
+
             @pl.when((z - d >= 0) & when)
             def _():
                 for s in subs:
@@ -190,11 +200,16 @@
         lax.fori_loop(first, last, body, 0)
 
     us, ds = range(usubs), range(dsubs)
-    held_right, held_left = zi == 0, zi == group - 1
-    right(up_copy, 1, 2, us[:1])
-    left(up_copy, 1, sp, us)
-    left(down_copy, 1, sp, ds, zi != group - 1)
-    left(down_copy, 1, 2, ds[: dsubs // 2], held_left)
+    far_right, far_left = z + 2 < sp, z - 2 >= 0
+    held_right = (zi == 0) & far_right
+    held_left = (zi == group - 1) & far_left
+    free_right = (zi != 0) | (z + 2 >= sp)
+    free_left = (zi != group - 1) | (z - 2 < 0)
+    right(up_copy, 1, 2, us[:1], z > 0)
+    away_left, away_right = zi != group - 1, zi != 0
+    left(up_copy, 1, 2, us)
+    left(up_copy, 2, sp, us, zi == group - 1)
+    left(down_copy, 1, sp, ds, free_left & jnp.logical_not(away_left))
 
     def wo_copy(tt):
         return remote(wout_hbm, wo.at[t], wo_send.at[tt], wo_recv.at[t], there(g, z, tt))
@@ -293,11 +308,13 @@
         state_copy().start()
 
     def rest_of_sends():
-        right(up_copy, 1, 2, us[1:], z == 0)
+        right(up_copy, 1, 2, us, z == 0)
         right(up_copy, 2, sp, us)
-        right(down_copy, 1, sp, ds, zi != 0)
+        right(down_copy, 1, 2, ds[:rsubs], free_right & (z == 0))
+        right(down_copy, 1, 2, ds[rsubs:], free_right & (zi == 0))
 
     right(up_copy, 1, 2, us[1:], z > 0)
+    right(down_copy, 1, 2, ds[:rsubs], free_right & (zi == 0) & (z > 0))
 
     @pl.when((z == 0) & (sp > 1))
     def _():
@@ -356,12 +373,6 @@
             gates[at, cols] = gain * (1.0 / (1.0 + jnp.exp(-ob[at, cols].astype(F32))))
 
     take_state(z > 1)
-    if sp > 1:
-        relay_up(1)
-    for j in range(1, half):
-        wo_arrived(lax.rem(x + j, half) * 2 + core).wait_recv()
-        wo_pass(j).start()
-
     for h in range(heads):
         cols = pl.ds(h * dh, dh)
         memory = st_in[h, :dh, :]
@@ -390,6 +401,25 @@
     for j in range(1, tp):
         mixed_copy(j).start()
     mixin[t] = mixed[pl.ds(aligned(t * rows, 16), rows), :]
+    left(up_copy, 2, sp, us, away_left)
+    def relays_up(first, last):
+        def body(k, _):
+            relay_up(k)
+            return 0
+
+        lax.fori_loop(first, last, body, 0)
+
+    def relays_down(k):
+        for c in range(pieces):
+            relay_down(k, c)
+
+    middle = min(sp, 2 + (sp - 2) // 2)
+    relays_up(1, min(2, sp))
+
+    for j in range(1, half):
+        wo_arrived(lax.rem(x + j, half) * 2 + core).wait_recv()
+        wo_pass(j).start()
+
     own[0].wait()
     loads[4].wait()
     for j in range(1, half):
@@ -417,35 +447,51 @@
         ntok[mine, :, at] = (mid[:, at].astype(F32) * factor * fgain_ref[:, at]).astype(BF16)
 
     def slot_of(xx, zz):
-        return core * same + xx * group + zz
-
-    def token(slot, send, where):
-        return remote(ntok.at[slot], ntok.at[slot], send, t_recv.at[slot], where)
-
-    def to_pair():
-        return token(mine, tz_send, there(g, other, t))
-
-    def to_x(j):
-        return token(mine, tx_send.at[j], there(g, z, lax.rem(x + j, half) * 2 + core))
-
-    def pass_x(j):
-        return token(slot_of(x, 1 - zi), tr_send.at[j], there(g, z, lax.rem(x + j, half) * 2 + core))
-
-    def to_partner(xx, zz):
-        slot = slot_of(xx, zz)
-        return token(slot, f_send.at[xx * group + zz], there(g, z, partner))
-
-    def arrived(slot):
-        return token(slot, tz_send, there(g, z, partner))
-
-    if group > 1:
-        to_pair().start()
+        return core * same + zz * half + xx
+
+    def token(slot, s, send, where):
+        at = ntok.at[slot, pl.ds(s * trows, trows), :]
+        return remote(at, at, send, t_recv.at[slot, s], where)
+
+    def to_pair(s):
+        return token(mine, s, tz_send.at[s], there(g, other, t))
+
+    def to_x(j, s):
+        return token(mine, s, tx_send.at[j, s], there(g, z, lax.rem(x + j, half) * 2 + core))
+
+    def pass_x(j, s):
+        where = there(g, z, lax.rem(x + j, half) * 2 + core)
+        return token(slot_of(x, 1 - zi), s, tr_send.at[j, s], where)
+
+    def to_partner(xx, zz, s):
+        return token(slot_of(xx, zz), s, f_send.at[zz * half + xx, s], there(g, z, partner))
+
+    def arrived(slot, s):
+        return token(slot, s, tz_send.at[s], there(g, z, partner))
+
+    ts = range(tsubs)
+
+    def give(xx, zz):
+        for s in ts:
+            to_partner(xx, zz, s).start()
+
+    def take(slot):
+        for s in ts:
+            arrived(slot, s).wait_recv()
+
+    for s in ts:
+        if group > 1:
+            to_pair(s).start()
     for j in range(1, half):
-        to_x(j).start()
-    to_partner(x, zi).start()
-    left(down_copy, 1, 2, ds[dsubs // 2 :], held_left)
-    left(down_copy, 2, sp, ds, held_left)
-    right(down_copy, 1, sp, ds, held_right)
+        for s in ts:
+            to_x(j, s).start()
+    give(x, zi)
+    left(down_copy, 1, sp, ds, away_left)
+    right(down_copy, 1, sp, ds, away_right)
+    left(down_copy, 1, 2, ds, held_left)
+    right(down_copy, 1, 2, ds, held_right)
+    left(down_copy, 2, sp, ds, held_left, flip=True)
+    right(down_copy, 2, sp, ds, held_right, flip=True)
 
     def relays_up(first, last):
         def body(k, _):
@@ -454,18 +500,31 @@
 
         lax.fori_loop(first, last, body, 0)
 
-    middle = 2 + (sp - 2) // 2
-    relays_up(2, middle)
+    @pl.when(edge)
+    def _():
+        relays_up(2, middle)
+
+    @pl.when(jnp.logical_not(edge))
+    def _():
+        relays_up(2, sp)
+
     for j in range(1, half):
         xx = lax.rem(x + j, half)
-        arrived(slot_of(xx, zi)).wait_recv()
-        to_partner(xx, zi).start()
+        take(slot_of(xx, zi))
+        give(xx, zi)
+
+    @pl.when(edge)
+    def _():
+        relays_up(middle, sp)
+        if sp > 1:
+            relays_down(1)
+
     if group > 1:
-        arrived(slot_of(x, 1 - zi)).wait_recv()
-        for j in range(1, half):
-            pass_x(j).start()
-        to_partner(x, 1 - zi).start()
-    relays_up(middle, sp)
+        for s in ts:
+            arrived(slot_of(x, 1 - zi), s).wait_recv()
+            for j in range(1, half):
+                pass_x(j, s).start()
+        give(x, 1 - zi)
     own[1].wait()
 
     def all_up(k, _):
@@ -473,28 +532,47 @@
         return 0
 
     lax.fori_loop(1, sp, all_up, 0)
-    if group > 1:
-        for j in range(1, half):
-            xx = lax.rem(x + j, half)
-            arrived(slot_of(xx, 1 - zi)).wait_recv()
-            to_partner(xx, 1 - zi).start()
-
-    def up_half(side):
-        def up_step(i, _):
-            at = pl.ds(side * same + i * 2, 2)
-            value = ntok[at].reshape(2 * rows, width)
-            y = jnp.dot(value, upw[...].reshape(width, part), preferred_element_type=F32)
-            y = jnp.maximum(y, 0.0)
-            act[at] = (y * y).astype(BF16).reshape(2, rows, part)
-            return 0
-
-        lax.fori_loop(0, same // 2, up_step, 0)
-
-    up_half(core)
-    for xx in range(half):
-        for zz in range(group):
-            arrived((1 - core) * same + xx * group + zz).wait_recv()
-    up_half(1 - core)
+
+    def up_quarter(side, zz):
+        at = pl.ds(side * same + zz * half, half)
+        value = ntok[at].reshape(half * rows, width)
+        y = jnp.dot(value, upw[...].reshape(width, part), preferred_element_type=F32)
+        y = jnp.maximum(y, 0.0)
+        act[at] = (y * y).astype(BF16).reshape(half, rows, part)
+
+    def up_step(i, _):
+        side = core + (1 - 2 * core) * lax.rem(i, 2)
+        zz = zi + (1 - 2 * zi) * (i // 2)
+
+        @pl.when(i == 1)
+        def _():
+            for xx in range(half):
+                take((1 - core) * same + zi * half + xx)
+
+        if group > 1:
+            @pl.when(i == 2)
+            def _():
+                for j in range(1, half):
+                    xx = lax.rem(x + j, half)
+                    take(slot_of(xx, 1 - zi))
+                    give(xx, 1 - zi)
+
+            @pl.when(i == 3)
+            def _():
+                for xx in range(half):
+                    take((1 - core) * same + (1 - zi) * half + xx)
+
+        up_quarter(side, zz)
+        return 0
+
+    lax.fori_loop(0, 2 * group, up_step, 0)
+    early = min(3, sp)
+
+    @pl.when(jnp.logical_not(edge))
+    def _():
+        for k in range(1, early):
+            relays_down(k)
+
     own[2].wait()
 
     def pre_copy(unit):
@@ -505,7 +583,7 @@
     def x_copy(unit, j):
         xx = lax.rem(x + j, half)
         return remote(
-            msend.at[unit, pl.ds(xx * group, group)], xrecv.at[unit, x],
+            msend.at[unit, :, xx], xrecv.at[unit, x],
             x_send.at[unit, j], x_recv.at[unit, x], there(g, z, xx * 2 + core),
         )
 
@@ -516,29 +594,25 @@
     def z_copy(unit):
         return remote(zsend.at[unit], zrecv.at[unit], z_send.at[unit], z_recv.at[unit], there(g, other, t))
 
-    def multiply(m, c):
-        k, parity = m // pieces, lax.rem(m, 2)
-        o = nth(k)
-        unit = o * pieces + c
-
+    def multiply(unit, o, c):
         def product(side):
             value = act[pl.ds(side * same, same)].reshape(same * rows, part)
             return jnp.dot(value, dnw[o, :, c * n : (c + 1) * n], preferred_element_type=F32)
 
         psend[unit] = product(1 - core).astype(BF16).reshape(psend.shape[1:])
         pre_copy(unit).start()
-        own_acc[parity] = product(core).reshape(psend.shape[1:])
+        own_acc[...] = product(core).reshape(own_acc.shape)
 
     def unit_of(m):
         return nth(m // pieces) * pieces + lax.rem(m, pieces)
 
-    def spread(m):
-        unit = unit_of(m)
+    def spread(unit):
         pre_copy(unit).wait_recv()
-        msend[unit] = (own_acc[lax.rem(m, 2)] + precv[unit].astype(F32)).astype(BF16)
+        msend[unit] = (own_acc[...] + precv[unit].astype(F32)).astype(BF16).reshape(msend.shape[1:])
         for j in range(1, half):
             x_copy(unit, j).start()
-        xrecv[unit, x] = msend[unit, pl.ds(x * group, group)]
+        for zz in range(group):
+            xrecv[unit, x, zz] = msend[unit, zz, x]
 
     def gathered(unit, zz):
         total = xrecv[unit, 0, zz].astype(F32)
@@ -555,18 +629,22 @@
             z_copy(unit).start()
 
     def stage(k, _):
-        @pl.when(k > 0)
-        def _():
-            relay_down(k)
-            finish_down(k)
-
+        o = nth(k)
         for c in range(pieces):
             m = k * pieces + c
-            multiply(m, c)
-
-            @pl.when(m >= 1)
+
+            ahead, piece = (k, c + 1) if c + 1 < pieces else (k + 1, 0)
+
+            @pl.when((ahead >= jnp.where(edge, 2, early)) & (ahead < sp))
             def _():
-                spread(m - 1)
+                relay_down(ahead, piece)
+
+            @pl.when(k > 0)
+            def _():
+                finish_down(k, c)
+
+            multiply(o * pieces + c, o, c)
+            spread(o * pieces + c)
 
             @pl.when(m >= 2)
             def _():
@@ -576,7 +654,6 @@
 
     lax.fori_loop(0, sp, stage, 0)
     units = sp * pieces
-    spread(units - 1)
     if units > 1:
         hand_over(units - 2)
     hand_over(units - 1)
@@ -627,17 +704,19 @@
     for j in range(1, half):
         wo_copy(lax.rem(x + j, half) * 2 + core).wait_send()
         wo_pass(j).wait_send()
-        to_x(j).wait_send()
-        if group > 1:
-            pass_x(j).wait_send()
+        for s in ts:
+            to_x(j, s).wait_send()
+            if group > 1:
+                pass_x(j, s).wait_send()
     wo_copy(partner).wait_send()
     for j in range(1, tp):
         mixed_copy(j).wait_send()
-    if group > 1:
-        to_pair().wait_send()
-    for xx in range(half):
-        for zz in range(group):
-            to_partner(xx, zz).wait_send()
+    for s in ts:
+        if group > 1:
+            to_pair(s).wait_send()
+        for xx in range(half):
+            for zz in range(group):
+                to_partner(xx, zz, s).wait_send()
 
     @pl.when(z < sp - 1)
     def _():
@@ -661,8 +740,10 @@
     group = 2 if sp % 2 == 0 else 1
     part = hidden // group
     usubs = 2 if up_rows % (32 * grp) == 0 else 1
-    dsubs = 2
     pieces = 2 if out_cols % 256 == 0 else 1
+    rsubs = 2
+    dsubs = rsubs * pieces
+    tsubs = 4 if rows % 64 == 0 else 1
     half = tp // 2
     same = half * group
     layer = tp * group
@@ -674,7 +755,7 @@
     dma = pltpu.SemaphoreType.DMA
     return pl.pallas_call(
         functools.partial(
-            kernel, (grp, sp, tp, heads, blocks, rows, group, usubs, dsubs, pieces)
+            kernel, (grp, sp, tp, heads, blocks, rows, group, usubs, rsubs, pieces, tsubs)
         ),
         out_shape=jax.ShapeDtypeStruct((rows, width), BF16),
         in_specs=[hbm] * 4 + [vmem] * 4 + [hbm] * 2 + [vmem] + [hbm] * 2,
@@ -695,11 +776,11 @@
             pltpu.VMEM((layer, rows, part), BF16),
             pltpu.VMEM((units, same, rows, n), BF16),
             pltpu.VMEM((units, same, rows, n), BF16),
-            pltpu.VMEM((units, same, rows, n), BF16),
+            pltpu.VMEM((units, group, half, rows, n), BF16),
             pltpu.VMEM((units, half, group, rows, n), BF16),
             pltpu.VMEM((units, rows, n), BF16),
             pltpu.VMEM((units, rows, n), BF16),
-            pltpu.VMEM((2, same, rows, n), F32),
+            pltpu.VMEM((same, rows, n), F32),
             pltpu.VMEM((units, rows, n) if n % 128 else (1, 8, 128), F32),
             pltpu.VMEM((heads, blocks, dh, BLOCK), BF16),
             pltpu.VMEM((heads, blocks, dh, dh), F32),
@@ -723,11 +804,11 @@
             dma,
             dma((tp,)),
             dma((tp,)),
-            dma((layer,)),
-            dma,
-            dma((half,)),
-            dma((half,)),
-            dma((same,)),
+            dma((layer, tsubs)),
+            dma((tsubs,)),
+            dma((half, tsubs)),
+            dma((half, tsubs)),
+            dma((same, tsubs)),
             dma((units,)),
             dma((units,)),
             dma((units, half)),

time: 162 us -> 120 us (0.74)
  Pallas kernels: 159 us -> 118 us
    pallas_call x1, Pallas kernels: 159 us -> 118 us  [shards(): pl.pallas_call(functools.partial(kernel, (grp, sp, tp, heads, blocks, row...]
where the time goes in v2:
time: 120 us
  Pallas kernels  118 us (98%)
  local copies, waits for them, and re-layouts  1.88 us (2%)
    pallas_call x1, Pallas kernels, shards(): pl.pallas_call(functools.partial(kernel, (grp, sp, tp, heads, blocks, row...  118 us

profile of v2, /device:TPU:17, one launch (start us, length us, event | category | flops | bytes accessed | tf_op | source)
XLA Modules:
  0.0 119.7 jit_solution(11254952649609454672)
XLA Ops:
  0.0 117.8 %shard_map.127 = bf16[128,2048]{1,0:T(8,128)(2,1)} custom-call(bf16[512,256]{1,0:T(8,128)(2,1)} %q_hbm.1, bf16[512,256]{1,0:T(8,128)(2,1)} %k_hbm.1, bf16[512,256]{1,0:T(8,128)(2,1)} %v_hbm.1, bf16[512,256]{1,0:T(8,128)(2,1)} %o_hbm.1, f32[2,512]{1,0:T(2,128)} %igate_ref.1, f32[2,512]{1,0:T(2,128)} %fgate_ref.1, f32[2,512]{1,0:T(2,128)} %extra_ref.1, ...), custom_call_target="tpu_custom_call" | custom-call | tf_op jit(solution)/shard_map/pallas_call | solution.py:756
  117.8 1.9 %copy.15 = bf16[128,2048]{1,0:T(8,128)(2,1)} copy(bf16[128,2048]{1,0:T(8,128)(2,1)} %shard_map.127) | data formatting | bytes 1048576

commit v3 on v2

--- a/solution.py
+++ b/solution.py
@@ -33,16 +33,17 @@
 
 def kernel(
     dims,
-    q_hbm, k_hbm, v_hbm, o_hbm, igate_ref, fgate_ref, extra_ref, hgain_ref, wout_hbm, res_hbm,
-    fgain_ref, up_hbm, down_hbm,
+    q_hbm, k_hbm, v_hbm, o_hbm, igate_hbm, fgate_hbm, extra_hbm, hgain_hbm, wout_hbm, res_hbm,
+    fgain_hbm, up_hbm, down_hbm,
     out_ref,
+    igate_ref, fgate_ref, extra_ref, hgain_ref, fgain_ref,
     qb, kb, vb, ob, resb, upw, dnw, wo, mixed, mixin, mid, ntok, act, psend, precv, msend, xrecv, zsend, zrecv,
-    own_acc, mlp, keyt, memp, hloc, gates, cols_ref, st_out, st_in,
+    acc, mlp, keyt, memp, hloc, gates, cols_ref, st_loc, st_out, st_in, top_out, top_in,
     in_sem, loc_sem, wu_send, wu_recv, wuy_send, wd_send, wd_recv, wdy_send, wo_send, wo_recv, wop_send,
     st_send, st_recv, mx_send, mx_recv, t_recv, tz_send, tx_send, tr_send, f_send,
     p_send, p_recv, x_send, x_recv, z_send, z_recv,
 ):
-    grp, sp, tp, heads, blocks, rows, group, usubs, rsubs, pieces, tsubs = dims
+    grp, sp, tp, heads, blocks, rows, group, usubs, rsubs, pieces, tsubs, parts = dims
     g, z, t = lax.axis_index("grp"), lax.axis_index("sp"), lax.axis_index("tp")
     half = tp // 2
     core, x = lax.rem(t, 2), t // 2
@@ -58,6 +59,7 @@
     up_rows = upw.shape[1]
     out_cols = dnw.shape[2]
     n = out_cols // pieces
+    w = n // parts
     urows = up_rows // grp // usubs
     drows = part // grp // rsubs
     trows = rows // tsubs
@@ -88,7 +90,10 @@
         return pltpu.make_async_copy(src, dst, in_sem.at[i])
 
     loads = [load(i, s, d) for i, (s, d) in enumerate(
-        ((k_hbm, kb), (v_hbm, vb), (q_hbm, qb), (o_hbm, ob), (res_hbm, resb))
+        (
+            (k_hbm, kb), (v_hbm, vb), (q_hbm, qb), (o_hbm, ob), (res_hbm, resb), (fgate_hbm, fgate_ref),
+            (extra_hbm, extra_ref), (igate_hbm, igate_ref), (hgain_hbm, hgain_ref), (fgain_hbm, fgain_ref),
+        )
     )]
     for c in loads:
         c.start()
@@ -245,6 +250,8 @@
             pieces_of.append(jnp.zeros((pad, BLOCK), F32))
         return jnp.concatenate(pieces_of, axis=0)
 
+    for i in (5, 6, 7):
+        loads[i].wait()
     pre = fgate_ref[...]
     log_forget = jnp.minimum(pre, 0.0) - jnp.log1p(jnp.exp(-jnp.abs(pre))) + extra_ref[...]
     cum_row = stacked(log_forget)
@@ -284,28 +291,34 @@
                     new,
                     jnp.exp(total + run[1] - new) * run[2] + jnp.exp(tail_max - new) * mem,
                 )
-        st_out[h, :dh, :] = run[2]
-        st_out[h, dh : dh + 8, :] = jnp.broadcast_to(run[1], (8, dh))
-        st_out[h, dh + 8 : dh + 16, :] = jnp.broadcast_to(run[0], (8, dh))
-
-    def state_copy():
-        return remote(st_out, st_in, st_send, st_recv, there(g, z + 1, t))
+        st_loc[h, :dh, :] = run[2]
+        st_loc[h, dh : dh + 8, :] = jnp.broadcast_to(run[1], (8, dh))
+        st_loc[h, dh + 8 : dh + 16, :] = jnp.broadcast_to(run[0], (8, dh))
+
+    def state_copies():
+        return (
+            remote(top_out, top_in, st_send.at[0], st_recv.at[0], there(g, z + 1, t)),
+            remote(st_out, st_in, st_send.at[1], st_recv.at[1], there(g, z + 1, t)),
+        )
 
     @pl.when(z == 0)
     def _():
         st_in[...] = jnp.zeros_like(st_in)
+        top_in[...] = jnp.zeros_like(top_in)
 
     def state_on():
         for h in range(heads):
-            m_in = st_in[h, dh : dh + 1, :]
-            m_loc = st_out[h, dh : dh + 1, :]
-            total = st_out[h, dh + 8 : dh + 9, :]
+            m_in = top_in[h, :1, :]
+            m_loc = st_loc[h, dh : dh + 1, :]
+            total = st_loc[h, dh + 8 : dh + 9, :]
             new = jnp.maximum(total + m_in, m_loc)
-            st_out[h, :dh, :] = (
-                jnp.exp(total + m_in - new) * st_in[h, :dh, :] + jnp.exp(m_loc - new) * st_out[h, :dh, :]
-            )
-            st_out[h, dh : dh + 8, :] = jnp.broadcast_to(new, (8, dh))
-        state_copy().start()
+            st_out[h] = (
+                jnp.exp(total + m_in - new) * st_in[h].astype(F32)
+                + jnp.exp(m_loc - new) * st_loc[h, :dh, :]
+            ).astype(BF16)
+            top_out[h] = jnp.broadcast_to(new, (8, dh))
+        for copy in state_copies():
+            copy.start()
 
     def rest_of_sends():
         right(up_copy, 1, 2, us, z == 0)
@@ -329,12 +342,14 @@
     causal = lax.broadcasted_iota(jnp.int32, (BLOCK, BLOCK), 0) >= lax.broadcasted_iota(
         jnp.int32, (BLOCK, BLOCK), 1
     )
+    loads[8].wait()
     gain = hgain_ref[...]
 
     def take_state(when):
         @pl.when(when)
         def _():
-            state_copy().wait_recv()
+            for copy in state_copies():
+                copy.wait_recv()
 
             @pl.when(z < sp - 1)
             def _():
@@ -372,19 +387,23 @@
             cols_ref[at, 2 * h + 1 : 2 * h + 2] = base
             gates[at, cols] = gain * (1.0 / (1.0 + jnp.exp(-ob[at, cols].astype(F32))))
 
+    if sp > 1:
+        @pl.when(z > 1)
+        def _():
+            relay_up(1)
+
     take_state(z > 1)
     for h in range(heads):
         cols = pl.ds(h * dh, dh)
-        memory = st_in[h, :dh, :]
-        stab = st_in[h, dh : dh + 1, 0:1]
+        memory = st_in[h]
+        stab = top_in[h, 0:1, 0:1]
         for b in range(blocks):
             at = pl.ds(b * BLOCK, BLOCK)
             local_max = cols_ref[at, 2 * h : 2 * h + 1]
             carry = cols_ref[at, 2 * h + 1 : 2 * h + 2] + stab
             row_max = jnp.maximum(local_max, carry)
-            hidden = jnp.exp(local_max - row_max) * hloc[at, cols] + jnp.exp(carry - row_max) * split_dot(
-                qb[at, cols], memory
-            )
+            past = jnp.dot(qb[at, cols], memory, preferred_element_type=F32)
+            hidden = jnp.exp(local_max - row_max) * hloc[at, cols] + jnp.exp(carry - row_max) * past
             mean_sq = jnp.mean(hidden * hidden, axis=1, keepdims=True)
             mixed[at, cols] = (hidden * lax.rsqrt(mean_sq + EPS) * gates[at, cols]).astype(BF16)
 
@@ -414,7 +433,10 @@
             relay_down(k, c)
 
     middle = min(sp, 2 + (sp - 2) // 2)
-    relays_up(1, min(2, sp))
+    if sp > 1:
+        @pl.when(z <= 1)
+        def _():
+            relay_up(1)
 
     for j in range(1, half):
         wo_arrived(lax.rem(x + j, half) * 2 + core).wait_recv()
@@ -422,6 +444,7 @@
 
     own[0].wait()
     loads[4].wait()
+    loads[9].wait()
     for j in range(1, half):
         wo_arrived(lax.rem(x + j, half) * 2 + 1 - core).wait_recv()
     wo_arrived(partner).wait_recv()
@@ -502,6 +525,8 @@
 
     @pl.when(edge)
     def _():
+        if sp > 1:
+            relay_down(1, 0)
         relays_up(2, middle)
 
     @pl.when(jnp.logical_not(edge))
@@ -517,7 +542,8 @@
     def _():
         relays_up(middle, sp)
         if sp > 1:
-            relays_down(1)
+            for c in range(1, pieces):
+                relay_down(1, c)
 
     if group > 1:
         for s in ts:
@@ -575,67 +601,105 @@
 
     own[2].wait()
 
-    def pre_copy(unit):
+    def pre_copy(unit, h):
         return remote(
-            psend.at[unit], precv.at[unit], p_send.at[unit], p_recv.at[unit], there(g, z, partner)
+            psend.at[unit, h], precv.at[unit, h], p_send.at[unit, h], p_recv.at[unit, h], there(g, z, partner)
         )
 
-    def x_copy(unit, j):
+    def x_copy(unit, h, j, zz):
         xx = lax.rem(x + j, half)
         return remote(
-            msend.at[unit, :, xx], xrecv.at[unit, x],
-            x_send.at[unit, j], x_recv.at[unit, x], there(g, z, xx * 2 + core),
+            msend.at[unit, h, zz, xx], xrecv.at[unit, h, x, zz],
+            x_send.at[unit, h, j, zz], x_recv.at[unit, h, x, zz], there(g, z, xx * 2 + core),
         )
 
-    def x_arrived(unit, xx):
-        at = xrecv.at[unit, xx]
-        return remote(at, at, x_send.at[unit, 0], x_recv.at[unit, xx], there(g, z, partner))
-
-    def z_copy(unit):
-        return remote(zsend.at[unit], zrecv.at[unit], z_send.at[unit], z_recv.at[unit], there(g, other, t))
+    def x_wait(unit, h, zz):
+        for j in range(1, half):
+            xx = lax.rem(x + j, half)
+            at = xrecv.at[unit, h, xx, zz]
+            remote(
+                at, at, x_send.at[unit, h, 0, zz], x_recv.at[unit, h, xx, zz], there(g, z, partner)
+            ).wait_recv()
+
+    def z_copy(unit, h):
+        return remote(
+            zsend.at[unit, h], zrecv.at[unit, h], z_send.at[unit, h], z_recv.at[unit, h], there(g, other, t)
+        )
+
+    share = part // grp
+
+    def product(side, o, c, which):
+        at = pl.ds(aligned(which * share, 128), share)
+        value = act[pl.ds(side * same, same), :, at].reshape(same * rows, share)
+        return jnp.dot(value, dnw[o, at, c * n : (c + 1) * n], preferred_element_type=F32)
+
+    def begin(o, c):
+        for side in range(2):
+            acc[side] = product(jnp.where(side == 0, 1 - core, core), o, c, g)
 
     def multiply(unit, o, c):
-        def product(side):
-            value = act[pl.ds(side * same, same)].reshape(same * rows, part)
-            return jnp.dot(value, dnw[o, :, c * n : (c + 1) * n], preferred_element_type=F32)
-
-        psend[unit] = product(1 - core).astype(BF16).reshape(psend.shape[1:])
-        pre_copy(unit).start()
-        own_acc[...] = product(core).reshape(own_acc.shape)
+        def rest(side, place):
+            total = acc[place]
+            for j in range(1, grp):
+                total = total + product(side, o, c, lax.rem(g + j, grp))
+            return total
+
+        total = rest(1 - core, 0).astype(BF16)
+        for h in range(parts):
+            psend[unit, h] = total[:, h * w : (h + 1) * w].reshape(psend.shape[2:])
+            pre_copy(unit, h).start()
+        acc[1] = rest(core, 1)
 
     def unit_of(m):
         return nth(m // pieces) * pieces + lax.rem(m, pieces)
 
     def spread(unit):
-        pre_copy(unit).wait_recv()
-        msend[unit] = (own_acc[...] + precv[unit].astype(F32)).astype(BF16).reshape(msend.shape[1:])
-        for j in range(1, half):
-            x_copy(unit, j).start()
-        for zz in range(group):
-            xrecv[unit, x, zz] = msend[unit, zz, x]
-
-    def gathered(unit, zz):
-        total = xrecv[unit, 0, zz].astype(F32)
+        for h in range(parts):
+            pre_copy(unit, h).wait_recv()
+            total = acc[1, :, h * w : (h + 1) * w].reshape(precv.shape[2:]) + precv[unit, h].astype(F32)
+            msend[unit, h] = total.astype(BF16).reshape(msend.shape[2:])
+            if group > 1:
+                for j in range(1, half):
+                    x_copy(unit, h, j, 1 - zi).start()
+        for h in range(parts):
+            for j in range(1, half):
+                x_copy(unit, h, j, zi).start()
+            for zz in range(group):
+                xrecv[unit, h, x, zz] = msend[unit, h, zz, x]
+
+    def gathered(unit, h, zz):
+        total = xrecv[unit, h, 0, zz].astype(F32)
         for xx in range(1, half):
-            total = total + xrecv[unit, xx, zz].astype(F32)
+            total = total + xrecv[unit, h, xx, zz].astype(F32)
         return total
 
     def hand_over(m):
         unit = unit_of(m)
-        for j in range(1, half):
-            x_arrived(unit, lax.rem(x + j, half)).wait_recv()
         if group > 1:
-            zsend[unit] = gathered(unit, 1 - zi).astype(BF16)
-            z_copy(unit).start()
+            for h in range(parts):
+                x_wait(unit, h, 1 - zi)
+                zsend[unit, h] = gathered(unit, h, 1 - zi).astype(BF16)
+                z_copy(unit, h).start()
 
     def stage(k, _):
         o = nth(k)
+        if early > 2:
+            for c in range(pieces):
+                @pl.when(edge & (k == c))
+                def _():
+                    relay_down(2, c)
+
+        @pl.when((k >= early) & edge)
+        def _():
+            relays_down(k)
+
         for c in range(pieces):
             m = k * pieces + c
 
+            begin(o, c)
             ahead, piece = (k, c + 1) if c + 1 < pieces else (k + 1, 0)
 
-            @pl.when((ahead >= jnp.where(edge, 2, early)) & (ahead < sp))
+            @pl.when((ahead >= early) & (ahead < sp) & jnp.logical_not(edge))
             def _():
                 relay_down(ahead, piece)
 
@@ -662,15 +726,17 @@
 
     def finish(m, _):
         unit = unit_of(m)
-        total = gathered(unit, zi)
-        if group > 1:
-            z_copy(unit).wait_recv()
-            total = total + zrecv[unit].astype(F32)
-        if direct:
-            at = pl.ds(aligned(unit * n, 128), n)
-            out_ref[:, at] = (mid[:, at].astype(F32) + total).astype(BF16)
-        else:
-            mlp[unit] = total
+        for h in range(parts):
+            x_wait(unit, h, zi)
+            total = gathered(unit, h, zi)
+            if group > 1:
+                z_copy(unit, h).wait_recv()
+                total = total + zrecv[unit, h].astype(F32)
+            if direct:
+                at = pl.ds(aligned(unit * n + h * w, 128), w)
+                out_ref[:, at] = (mid[:, at].astype(F32) + total).astype(BF16)
+            else:
+                mlp[unit] = total
         return 0
 
     lax.fori_loop(0, units, finish, 0)
@@ -693,11 +759,13 @@
 
         for c in range(pieces):
             unit = o * pieces + c
-            pre_copy(unit).wait_send()
-            for j in range(1, half):
-                x_copy(unit, j).wait_send()
-            if group > 1:
-                z_copy(unit).wait_send()
+            for h in range(parts):
+                pre_copy(unit, h).wait_send()
+                for j in range(1, half):
+                    for zz in range(group):
+                        x_copy(unit, h, j, zz).wait_send()
+                if group > 1:
+                    z_copy(unit, h).wait_send()
         return 0
 
     lax.fori_loop(0, sp, drain, 0)
@@ -720,7 +788,8 @@
 
     @pl.when(z < sp - 1)
     def _():
-        state_copy().wait_send()
+        for copy in state_copies():
+            copy.wait_send()
 
 
 def shards(
@@ -741,7 +810,7 @@
     part = hidden // group
     usubs = 2 if up_rows % (32 * grp) == 0 else 1
     pieces = 2 if out_cols % 256 == 0 else 1
-    rsubs = 2
+    rsubs = 4 if part % (64 * grp) == 0 else 1
     dsubs = rsubs * pieces
     tsubs = 4 if rows % 64 == 0 else 1
     half = tp // 2
@@ -749,18 +818,25 @@
     layer = tp * group
     units = sp * pieces
     n = out_cols // pieces
+    parts = 2 if n % 256 == 0 else 1
+    w = n // parts
 
     vmem = pl.BlockSpec(memory_space=pltpu.VMEM)
     hbm = pl.BlockSpec(memory_space=pl.ANY)
     dma = pltpu.SemaphoreType.DMA
     return pl.pallas_call(
         functools.partial(
-            kernel, (grp, sp, tp, heads, blocks, rows, group, usubs, rsubs, pieces, tsubs)
+            kernel, (grp, sp, tp, heads, blocks, rows, group, usubs, rsubs, pieces, tsubs, parts)
         ),
         out_shape=jax.ShapeDtypeStruct((rows, width), BF16),
-        in_specs=[hbm] * 4 + [vmem] * 4 + [hbm] * 2 + [vmem] + [hbm] * 2,
+        in_specs=[hbm] * 13,
         out_specs=vmem,
         scratch_shapes=[
+            pltpu.VMEM((heads, tokens), F32),
+            pltpu.VMEM((heads, tokens), F32),
+            pltpu.VMEM((heads, tokens), F32),
+            pltpu.VMEM((1, dh), F32),
+            pltpu.VMEM((1, width), F32),
             pltpu.VMEM((tokens, across), BF16),
             pltpu.VMEM((tokens, across), BF16),
             pltpu.VMEM((tokens, across), BF16),
@@ -774,13 +850,13 @@
             pltpu.VMEM((rows, width), BF16),
             pltpu.VMEM((layer, rows, width), BF16),
             pltpu.VMEM((layer, rows, part), BF16),
-            pltpu.VMEM((units, same, rows, n), BF16),
-            pltpu.VMEM((units, same, rows, n), BF16),
-            pltpu.VMEM((units, group, half, rows, n), BF16),
-            pltpu.VMEM((units, half, group, rows, n), BF16),
-            pltpu.VMEM((units, rows, n), BF16),
-            pltpu.VMEM((units, rows, n), BF16),
-            pltpu.VMEM((same, rows, n), F32),
+            pltpu.VMEM((units, parts, same, rows, w), BF16),
+            pltpu.VMEM((units, parts, same, rows, w), BF16),
+            pltpu.VMEM((units, parts, group, half, rows, w), BF16),
+            pltpu.VMEM((units, parts, half, group, rows, w), BF16),
+            pltpu.VMEM((units, parts, rows, w), BF16),
+            pltpu.VMEM((units, parts, rows, w), BF16),
+            pltpu.VMEM((2, same * rows, n), F32),
             pltpu.VMEM((units, rows, n) if n % 128 else (1, 8, 128), F32),
             pltpu.VMEM((heads, blocks, dh, BLOCK), BF16),
             pltpu.VMEM((heads, blocks, dh, dh), F32),
@@ -788,8 +864,11 @@
             pltpu.VMEM((tokens, across), F32),
             pltpu.VMEM((tokens, 128), F32),
             pltpu.VMEM((heads, dh + 16, dh), F32),
-            pltpu.VMEM((heads, dh + 16, dh), F32),
-            dma((5,)),
+            pltpu.VMEM((heads, dh, dh), BF16),
+            pltpu.VMEM((heads, dh, dh), BF16),
+            pltpu.VMEM((heads, 8, dh), F32),
+            pltpu.VMEM((heads, 8, dh), F32),
+            dma((10,)),
             dma((3,)),
             dma((sp, usubs)),
             dma((sp, grp, usubs)),
@@ -800,8 +879,8 @@
             dma((tp,)),
             dma((tp,)),
             dma((half,)),
-            dma,
-            dma,
+            dma((2,)),
+            dma((2,)),
             dma((tp,)),
             dma((tp,)),
             dma((layer, tsubs)),
@@ -809,12 +888,12 @@
             dma((half, tsubs)),
             dma((half, tsubs)),
             dma((same, tsubs)),
-            dma((units,)),
-            dma((units,)),
-            dma((units, half)),
-            dma((units, half)),
-            dma((units,)),
-            dma((units,)),
+            dma((units, parts)),
+            dma((units, parts)),
+            dma((units, parts, half, group)),
+            dma((units, parts, half, group)),
+            dma((units, parts)),
+            dma((units, parts)),
         ],
         compiler_params=pltpu.CompilerParams(
             collective_id=0, has_side_effects=True, vmem_limit_bytes=60 * 1024 * 1024

time: 120 us -> 116 us (0.967)
  Pallas kernels: 118 us -> 114 us
    pallas_call x1, Pallas kernels: 118 us -> 114 us  [shards(): pl.pallas_call(functools.partial(kernel, (grp, sp, tp, heads, blocks, row...]
where the time goes in v3:
time: 116 us
  Pallas kernels  114 us (98%)
  local copies, waits for them, and re-layouts  1.88 us (2%)
    pallas_call x1, Pallas kernels, shards(): pl.pallas_call(functools.partial(kernel, (grp, sp, tp, heads, blocks, row...  114 us

profile of v3, /device:TPU:17, one launch (start us, length us, event | category | flops | bytes accessed | tf_op | source)
XLA Modules:
  0.0 115.9 jit_solution(9570166449170154402)
XLA Ops:
  0.0 114.0 %shard_map.127 = bf16[128,2048]{1,0:T(8,128)(2,1)} custom-call(bf16[512,256]{1,0:T(8,128)(2,1)} %q_hbm.1, bf16[512,256]{1,0:T(8,128)(2,1)} %k_hbm.1, bf16[512,256]{1,0:T(8,128)(2,1)} %v_hbm.1, bf16[512,256]{1,0:T(8,128)(2,1)} %o_hbm.1, f32[2,512]{1,0:T(2,128)} %igate_hbm.1, f32[2,512]{1,0:T(2,128)} %fgate_hbm.1, f32[2,512]{1,0:T(2,128)} %extra_hbm.1, ...), custom_call_target="tpu_custom_call" | custom-call | tf_op jit(solution)/shard_map/pallas_call | solution.py:827
  114.0 1.9 %copy.15 = bf16[128,2048]{1,0:T(8,128)(2,1)} copy(bf16[128,2048]{1,0:T(8,128)(2,1)} %shard_map.127) | data formatting | bytes 1048576

commit v4 on v3

--- a/solution.py
+++ b/solution.py
@@ -36,11 +36,11 @@
     q_hbm, k_hbm, v_hbm, o_hbm, igate_hbm, fgate_hbm, extra_hbm, hgain_hbm, wout_hbm, res_hbm,
     fgain_hbm, up_hbm, down_hbm,
     out_ref,
-    igate_ref, fgate_ref, extra_ref, hgain_ref, fgain_ref,
-    qb, kb, vb, ob, resb, upw, dnw, wo, mixed, mixin, mid, ntok, act, psend, precv, msend, xrecv, zsend, zrecv,
+    gates_in, hgain_ref, fgain_ref, qkvo, resb,
+    upw, dnw, wo, mixed, mixin, mid, ntok, act, psend, precv, msend, xrecv, zsend, zrecv,
     acc, mlp, keyt, memp, hloc, gates, cols_ref, st_loc, st_out, st_in, top_out, top_in,
-    in_sem, loc_sem, wu_send, wu_recv, wuy_send, wd_send, wd_recv, wdy_send, wo_send, wo_recv, wop_send,
-    st_send, st_recv, mx_send, mx_recv, t_recv, tz_send, tx_send, tr_send, f_send,
+    in_sem, loc_sem, wu_send, wu_recv, uy_send, uy_recv, wd_send, wd_recv, dy_send, dy_recv,
+    wo_send, wo_recv, st_send, st_recv, mx_send, mx_recv, t_send, t_recv, tz_recv,
     p_send, p_recv, x_send, x_recv, z_send, z_recv,
 ):
     grp, sp, tp, heads, blocks, rows, group, usubs, rsubs, pieces, tsubs, parts = dims
@@ -86,17 +86,27 @@
             bit *= 2
         return total
 
-    def load(i, src, dst):
-        return pltpu.make_async_copy(src, dst, in_sem.at[i])
-
-    loads = [load(i, s, d) for i, (s, d) in enumerate(
-        (
-            (k_hbm, kb), (v_hbm, vb), (q_hbm, qb), (o_hbm, ob), (res_hbm, resb), (fgate_hbm, fgate_ref),
-            (extra_hbm, extra_ref), (igate_hbm, igate_ref), (hgain_hbm, hgain_ref), (fgain_hbm, fgain_ref),
-        )
-    )]
+    kb, vb, qb, ob = (qkvo.at[i] for i in range(4))
+
+    def await_recv(ref, sem):
+        remote(ref, ref, mx_send, sem, there(g, z, partner)).wait_recv()
+
+    def await_send(ref, sem):
+        remote(ref, ref, sem, mx_recv, there(g, z, partner)).wait_send()
+
+    loads = [
+        pltpu.make_async_copy(src, dst, in_sem.at[i])
+        for src, dst, i in (
+            (fgate_hbm, gates_in.at[0], 0), (extra_hbm, gates_in.at[1], 0), (igate_hbm, gates_in.at[2], 0),
+            (k_hbm, kb, 1), (v_hbm, vb, 1), (q_hbm, qb, 2), (o_hbm, ob, 2),
+            (hgain_hbm, hgain_ref, 3), (fgain_hbm, fgain_ref, 4), (res_hbm, resb, 5),
+        )
+    ]
     for c in loads:
         c.start()
+
+    def loaded(ref, i):
+        pltpu.make_async_copy(ref, ref, in_sem.at[i]).wait()
 
     barrier = pltpu.get_barrier_semaphore()
     for j in range(1, tp):
@@ -122,7 +132,7 @@
         return remote(
             up_hbm.at[up_rows_of(g, s), pl.ds(aligned(lax.rem(zz, group) * part, 128), part)],
             upw.at[z, up_rows_of(g, s), :],
-            wu_send.at[zz, s], wu_recv.at[z, g, s], there(g, zz, t),
+            wu_send, wu_recv.at[z, s], there(g, zz, t),
         )
 
     def down_copy(zz, s):
@@ -130,53 +140,41 @@
         return remote(
             down_hbm.at[pl.ds(aligned(first, 16), drows), pl.ds(s // rsubs * n, n)],
             dnw.at[(z, *down_at(g, s))],
-            wd_send.at[zz, s], wd_recv.at[z, g, s], there(g, zz, t),
+            wd_send, wd_recv.at[z, s], there(g, zz, t),
         )
 
     def up_pass(o, s, j):
         at = upw.at[o, up_rows_of(g, s), :]
-        return remote(at, at, wuy_send.at[o, s, j], wu_recv.at[o, g, s], there(lax.rem(g + j, grp), z, t))
+        return remote(at, at, uy_send, uy_recv, there(lax.rem(g + j, grp), z, t))
 
     def down_pass(o, s, j):
         at = dnw.at[(o, *down_at(g, s))]
-        return remote(at, at, wdy_send.at[o, s, j], wd_recv.at[o, g, s], there(lax.rem(g + j, grp), z, t))
-
-    def up_arrived(o, c, s):
-        at = upw.at[o, up_rows_of(c, s), :]
-        return remote(at, at, wuy_send.at[o, s, 0], wu_recv.at[o, c, s], there(g, z, t))
-
-    def down_arrived(o, c, s):
-        at = dnw.at[(o, *down_at(c, s))]
-        return remote(at, at, wdy_send.at[o, s, 0], wd_recv.at[o, c, s], there(g, z, t))
+        where = there(lax.rem(g + j, grp), z, t)
+        return remote(at, at, dy_send, dy_recv.at[o, s // rsubs, grp - j - 1], where)
+
+    def of_piece(c):
+        return range(c * rsubs, (c + 1) * rsubs)
 
     def relay_up(k):
         o = nth(k)
         for s in range(usubs):
-            up_arrived(o, g, s).wait_recv()
+            await_recv(upw.at[o, up_rows_of(g, s), :], wu_recv.at[o, s])
             for j in range(1, grp):
                 up_pass(o, s, j).start()
-
-    def of_piece(c):
-        return range(c * rsubs, (c + 1) * rsubs)
 
     def relay_down(k, c):
         o = nth(k)
         for s in of_piece(c):
-            down_arrived(o, g, s).wait_recv()
+            await_recv(dnw.at[(o, *down_at(g, s))], wd_recv.at[o, s])
             for j in range(1, grp):
                 down_pass(o, s, j).start()
 
-    def finish_up(k):
-        o = nth(k)
-        for s in range(usubs):
-            for j in range(1, grp):
-                up_arrived(o, lax.rem(g + j, grp), s).wait_recv()
-
     def finish_down(k, c):
         o = nth(k)
-        for s in of_piece(c):
-            for j in range(1, grp):
-                down_arrived(o, lax.rem(g + j, grp), s).wait_recv()
+        for j in range(1, grp):
+            first = aligned(lax.rem(g + j, grp) * (drows * rsubs), 16)
+            at = dnw.at[o, pl.ds(first, drows * rsubs), pl.ds(c * n, n)]
+            await_recv(at, dy_recv.at[o, c, j - 1])
 
     def right(copy, first, last, subs, when=True, flip=False):
         def body(i, _):
@@ -217,14 +215,14 @@
     left(down_copy, 1, sp, ds, free_left & jnp.logical_not(away_left))
 
     def wo_copy(tt):
-        return remote(wout_hbm, wo.at[t], wo_send.at[tt], wo_recv.at[t], there(g, z, tt))
+        return remote(wout_hbm, wo.at[t], wo_send, wo_recv.at[t], there(g, z, tt))
 
     def wo_pass(j):
         tt = lax.rem(x + j, half) * 2 + core
-        return remote(wo.at[tt], wo.at[tt], wop_send.at[j], wo_recv.at[tt], there(g, z, partner))
+        return remote(wo.at[tt], wo.at[tt], wo_send, wo_recv.at[tt], there(g, z, partner))
 
     def wo_arrived(tt):
-        return remote(wo.at[tt], wo.at[tt], wop_send.at[0], wo_recv.at[tt], there(g, z, partner))
+        await_recv(wo.at[tt], wo_recv.at[tt])
 
     for j in range(1, half):
         wo_copy(lax.rem(x + j, half) * 2 + core).start()
@@ -237,7 +235,7 @@
     for c in own:
         c.start()
 
-    dh = qb.shape[1] // heads
+    dh = qkvo.shape[2] // heads
     scale = dh ** (-0.5)
     count = heads * blocks
     pad = -count % 8
@@ -250,22 +248,20 @@
             pieces_of.append(jnp.zeros((pad, BLOCK), F32))
         return jnp.concatenate(pieces_of, axis=0)
 
-    for i in (5, 6, 7):
-        loads[i].wait()
-    pre = fgate_ref[...]
-    log_forget = jnp.minimum(pre, 0.0) - jnp.log1p(jnp.exp(-jnp.abs(pre))) + extra_ref[...]
+    loaded(gates_in, 0)
+    pre = gates_in[0]
+    log_forget = jnp.minimum(pre, 0.0) - jnp.log1p(jnp.exp(-jnp.abs(pre))) + gates_in[1]
     cum_row = stacked(log_forget)
     lane = lax.broadcasted_iota(jnp.int32, cum_row.shape, 1)
     step = 1
     while step < BLOCK:
         cum_row = cum_row + jnp.where(lane >= step, pltpu.roll(cum_row, step, 1), 0.0)
         step *= 2
-    rest_row = stacked(igate_ref[...]) - cum_row
+    rest_row = stacked(gates_in[2]) - cum_row
     cum_col = cum_row.T
     rest_col = rest_row.T
 
-    loads[0].wait()
-    loads[1].wait()
+    loaded(qkvo.at[pl.ds(0, 2)], 1)
     before, totals = {}, {}
     for h in range(heads):
         cols = pl.ds(h * dh, dh)
@@ -337,12 +333,11 @@
     def _():
         rest_of_sends()
 
-    loads[2].wait()
-    loads[3].wait()
+    loaded(qkvo.at[pl.ds(2, 2)], 2)
     causal = lax.broadcasted_iota(jnp.int32, (BLOCK, BLOCK), 0) >= lax.broadcasted_iota(
         jnp.int32, (BLOCK, BLOCK), 1
     )
-    loads[8].wait()
+    loaded(hgain_ref, 3)
     gain = hgain_ref[...]
 
     def take_state(when):
@@ -411,11 +406,8 @@
         d = lax.rem(t + j, tp)
         return remote(
             mixed.at[pl.ds(aligned(d * rows, 16), rows), :],
-            mixin.at[t], mx_send.at[j], mx_recv.at[t], there(g, z, d),
-        )
-
-    def mixed_arrived(tt):
-        return remote(mixin.at[tt], mixin.at[tt], mx_send.at[0], mx_recv.at[tt], there(g, z, partner))
+            mixin.at[t], mx_send, mx_recv, there(g, z, d),
+        )
 
     for j in range(1, tp):
         mixed_copy(j).start()
@@ -439,17 +431,16 @@
             relay_up(1)
 
     for j in range(1, half):
-        wo_arrived(lax.rem(x + j, half) * 2 + core).wait_recv()
+        wo_arrived(lax.rem(x + j, half) * 2 + core)
         wo_pass(j).start()
 
     own[0].wait()
-    loads[4].wait()
-    loads[9].wait()
+    loaded(fgain_ref, 4)
+    loaded(resb, 5)
     for j in range(1, half):
-        wo_arrived(lax.rem(x + j, half) * 2 + 1 - core).wait_recv()
-    wo_arrived(partner).wait_recv()
-    for j in range(1, tp):
-        mixed_arrived(lax.rem(t + j, tp)).wait_recv()
+        wo_arrived(lax.rem(x + j, half) * 2 + 1 - core)
+    wo_arrived(partner)
+    await_recv(mixin.at[pl.ds(0, tp - 1)], mx_recv)
 
     chunk = min(512, width)
     sum_sq = jnp.zeros((rows, 1), F32)
@@ -472,42 +463,36 @@
     def slot_of(xx, zz):
         return core * same + zz * half + xx
 
-    def token(slot, s, send, where):
-        at = ntok.at[slot, pl.ds(s * trows, trows), :]
-        return remote(at, at, send, t_recv.at[slot, s], where)
+    def row_part(slot, s):
+        return ntok.at[slot, pl.ds(s * trows, trows), :]
 
     def to_pair(s):
-        return token(mine, s, tz_send.at[s], there(g, other, t))
-
-    def to_x(j, s):
-        return token(mine, s, tx_send.at[j, s], there(g, z, lax.rem(x + j, half) * 2 + core))
+        at = row_part(mine, s)
+        return remote(at, at, t_send, tz_recv.at[s], there(g, other, t))
+
+    def to_x(j):
+        where = there(g, z, lax.rem(x + j, half) * 2 + core)
+        return remote(ntok.at[mine], ntok.at[mine], t_send, t_recv.at[mine], where)
 
     def pass_x(j, s):
-        where = there(g, z, lax.rem(x + j, half) * 2 + core)
-        return token(slot_of(x, 1 - zi), s, tr_send.at[j, s], where)
-
-    def to_partner(xx, zz, s):
-        return token(slot_of(xx, zz), s, f_send.at[zz * half + xx, s], there(g, z, partner))
-
-    def arrived(slot, s):
-        return token(slot, s, tz_send.at[s], there(g, z, partner))
+        slot = slot_of(x, 1 - zi)
+        at = row_part(slot, s)
+        return remote(at, at, t_send, t_recv.at[slot], there(g, z, lax.rem(x + j, half) * 2 + core))
+
+    def give(xx, zz):
+        slot = slot_of(xx, zz)
+        remote(ntok.at[slot], ntok.at[slot], t_send, t_recv.at[slot], there(g, z, partner)).start()
+
+    def take(slot):
+        await_recv(ntok.at[slot], t_recv.at[slot])
 
     ts = range(tsubs)
-
-    def give(xx, zz):
-        for s in ts:
-            to_partner(xx, zz, s).start()
-
-    def take(slot):
-        for s in ts:
-            arrived(slot, s).wait_recv()
 
     for s in ts:
         if group > 1:
             to_pair(s).start()
     for j in range(1, half):
-        for s in ts:
-            to_x(j, s).start()
+        to_x(j).start()
     give(x, zi)
     left(down_copy, 1, sp, ds, away_left)
     right(down_copy, 1, sp, ds, away_right)
@@ -547,17 +532,15 @@
 
     if group > 1:
         for s in ts:
-            arrived(slot_of(x, 1 - zi), s).wait_recv()
+            await_recv(row_part(slot_of(x, 1 - zi), s), tz_recv.at[s])
             for j in range(1, half):
                 pass_x(j, s).start()
         give(x, 1 - zi)
     own[1].wait()
 
-    def all_up(k, _):
-        finish_up(k)
-        return 0
-
-    lax.fori_loop(1, sp, all_up, 0)
+    others = up_rows - up_rows // grp
+    if sp > 1 and grp > 1:
+        await_recv(upw.at[pl.ds(0, sp - 1), pl.ds(0, others), :], uy_recv)
 
     def up_quarter(side, zz):
         at = pl.ds(side * same + zz * half, half)
@@ -603,27 +586,22 @@
 
     def pre_copy(unit, h):
         return remote(
-            psend.at[unit, h], precv.at[unit, h], p_send.at[unit, h], p_recv.at[unit, h], there(g, z, partner)
+            psend.at[unit, h], precv.at[unit, h], p_send, p_recv.at[unit, h], there(g, z, partner)
         )
 
     def x_copy(unit, h, j, zz):
         xx = lax.rem(x + j, half)
         return remote(
             msend.at[unit, h, zz, xx], xrecv.at[unit, h, x, zz],
-            x_send.at[unit, h, j, zz], x_recv.at[unit, h, x, zz], there(g, z, xx * 2 + core),
+            x_send, x_recv.at[unit, h, zz], there(g, z, xx * 2 + core),
         )
 
     def x_wait(unit, h, zz):
-        for j in range(1, half):
-            xx = lax.rem(x + j, half)
-            at = xrecv.at[unit, h, xx, zz]
-            remote(
-                at, at, x_send.at[unit, h, 0, zz], x_recv.at[unit, h, xx, zz], there(g, z, partner)
-            ).wait_recv()
+        await_recv(xrecv.at[unit, h, pl.ds(0, half - 1), zz], x_recv.at[unit, h, zz])
 
     def z_copy(unit, h):
         return remote(
-            zsend.at[unit, h], zrecv.at[unit, h], z_send.at[unit, h], z_recv.at[unit, h], there(g, other, t)
+            zsend.at[unit, h], zrecv.at[unit, h], z_send, z_recv.at[unit, h], there(g, other, t)
         )
 
     share = part // grp
@@ -745,46 +723,20 @@
             at = pl.ds(unit * n, n)
             out_ref[:, at] = (mid[:, at].astype(F32) + mlp[unit]).astype(BF16)
 
-    def drain(o, _):
-        @pl.when(o != z)
-        def _():
-            for s in us:
-                up_copy(o, s).wait_send()
-                for j in range(1, grp):
-                    up_pass(o, s, j).wait_send()
-            for s in ds:
-                down_copy(o, s).wait_send()
-                for j in range(1, grp):
-                    down_pass(o, s, j).wait_send()
-
-        for c in range(pieces):
-            unit = o * pieces + c
-            for h in range(parts):
-                pre_copy(unit, h).wait_send()
-                for j in range(1, half):
-                    for zz in range(group):
-                        x_copy(unit, h, j, zz).wait_send()
-                if group > 1:
-                    z_copy(unit, h).wait_send()
-        return 0
-
-    lax.fori_loop(0, sp, drain, 0)
-    for j in range(1, half):
-        wo_copy(lax.rem(x + j, half) * 2 + core).wait_send()
-        wo_pass(j).wait_send()
-        for s in ts:
-            to_x(j, s).wait_send()
-            if group > 1:
-                pass_x(j, s).wait_send()
-    wo_copy(partner).wait_send()
-    for j in range(1, tp):
-        mixed_copy(j).wait_send()
-    for s in ts:
-        if group > 1:
-            to_pair(s).wait_send()
-        for xx in range(half):
-            for zz in range(group):
-                to_partner(xx, zz, s).wait_send()
+    if sp > 1:
+        await_send(upw.at[pl.ds(0, sp - 1), pl.ds(0, up_rows // grp), :], wu_send)
+        await_send(dnw.at[pl.ds(0, sp - 1), pl.ds(0, part // grp), :], wd_send)
+        if grp > 1:
+            await_send(upw.at[pl.ds(0, sp - 1), pl.ds(0, others), :], uy_send)
+            await_send(dnw.at[pl.ds(0, sp - 1), pl.ds(0, part - share), :], dy_send)
+    await_send(wo.at[pl.ds(0, 2 * half - 1)], wo_send)
+    await_send(mixin.at[pl.ds(0, tp - 1)], mx_send)
+    await_send(ntok.at[pl.ds(0, group * (half - 1) + same + group - 1)], t_send)
+    await_send(psend, p_send)
+    if half > 1:
+        await_send(msend.at[:, :, :, pl.ds(0, half - 1)], x_send)
+    if group > 1:
+        await_send(zsend, z_send)
 
     @pl.when(z < sp - 1)
     def _():
@@ -832,15 +784,10 @@
         in_specs=[hbm] * 13,
         out_specs=vmem,
         scratch_shapes=[
-            pltpu.VMEM((heads, tokens), F32),
-            pltpu.VMEM((heads, tokens), F32),
-            pltpu.VMEM((heads, tokens), F32),
+            pltpu.VMEM((3, heads, tokens), F32),
             pltpu.VMEM((1, dh), F32),
             pltpu.VMEM((1, width), F32),
-            pltpu.VMEM((tokens, across), BF16),
-            pltpu.VMEM((tokens, across), BF16),
-            pltpu.VMEM((tokens, across), BF16),
-            pltpu.VMEM((tokens, across), BF16),
+            pltpu.VMEM((4, tokens, across), BF16),
             pltpu.VMEM((rows, width), BF16),
             pltpu.VMEM((sp, up_rows, part), BF16),
             pltpu.VMEM((sp, part, out_cols), BF16),
@@ -868,31 +815,30 @@
             pltpu.VMEM((heads, dh, dh), BF16),
             pltpu.VMEM((heads, 8, dh), F32),
             pltpu.VMEM((heads, 8, dh), F32),
-            dma((10,)),
+            dma((6,)),
             dma((3,)),
+            dma,
             dma((sp, usubs)),
-            dma((sp, grp, usubs)),
-            dma((sp, usubs, grp)),
+            dma,
+            dma,
+            dma,
             dma((sp, dsubs)),
-            dma((sp, grp, dsubs)),
-            dma((sp, dsubs, grp)),
+            dma,
+            dma((sp, pieces, grp)),
+            dma,
             dma((tp,)),
-            dma((tp,)),
-            dma((half,)),
             dma((2,)),
             dma((2,)),
-            dma((tp,)),
-            dma((tp,)),
-            dma((layer, tsubs)),
+            dma,
+            dma,
+            dma,
+            dma((layer,)),
             dma((tsubs,)),
-            dma((half, tsubs)),
-            dma((half, tsubs)),
-            dma((same, tsubs)),
+            dma,
             dma((units, parts)),
-            dma((units, parts)),
-            dma((units, parts, half, group)),
-            dma((units, parts, half, group)),
-            dma((units, parts)),
+            dma,
+            dma((units, parts, group)),
+            dma,
             dma((units, parts)),
         ],
         compiler_params=pltpu.CompilerParams(

time: 116 us -> 113 us (0.974)
  Pallas kernels: 114 us -> 111 us
    pallas_call x1, Pallas kernels: 114 us -> 111 us  [shards(): pl.pallas_call(functools.partial(kernel, (grp, sp, tp, heads, blocks, row...]
where the time goes in v4:
time: 113 us
  Pallas kernels  111 us (98%)
  local copies, waits for them, and re-layouts  1.88 us (2%)
    pallas_call x1, Pallas kernels, shards(): pl.pallas_call(functools.partial(kernel, (grp, sp, tp, heads, blocks, row...  111 us

profile of v4, /device:TPU:17, one launch (start us, length us, event | category | flops | bytes accessed | tf_op | source)
XLA Modules:
  0.0 112.6 jit_solution(13711947180904110063)
XLA Ops:
  0.0 110.7 %shard_map.127 = bf16[128,2048]{1,0:T(8,128)(2,1)} custom-call(bf16[512,256]{1,0:T(8,128)(2,1)} %q_hbm.1, bf16[512,256]{1,0:T(8,128)(2,1)} %k_hbm.1, bf16[512,256]{1,0:T(8,128)(2,1)} %v_hbm.1, bf16[512,256]{1,0:T(8,128)(2,1)} %o_hbm.1, f32[2,512]{1,0:T(2,128)} %igate_hbm.1, f32[2,512]{1,0:T(2,128)} %fgate_hbm.1, f32[2,512]{1,0:T(2,128)} %extra_hbm.1, ...), custom_call_target="tpu_custom_call" | custom-call | tf_op jit(solution)/shard_map/pallas_call | solution.py:779
  110.7 1.9 %copy.15 = bf16[128,2048]{1,0:T(8,128)(2,1)} copy(bf16[128,2048]{1,0:T(8,128)(2,1)} %shard_map.127) | data formatting | bytes 1048576

commit v5 on v4

--- a/solution.py
+++ b/solution.py
@@ -41,7 +41,7 @@
     acc, mlp, keyt, memp, hloc, gates, cols_ref, st_loc, st_out, st_in, top_out, top_in,
     in_sem, loc_sem, wu_send, wu_recv, uy_send, uy_recv, wd_send, wd_recv, dy_send, dy_recv,
     wo_send, wo_recv, st_send, st_recv, mx_send, mx_recv, t_send, t_recv, tz_recv,
-    p_send, p_recv, x_send, x_recv, z_send, z_recv,
+    p_send, p_recv, x_send, x_recv, x_home, z_send, z_recv,
 ):
     grp, sp, tp, heads, blocks, rows, group, usubs, rsubs, pieces, tsubs, parts = dims
     g, z, t = lax.axis_index("grp"), lax.axis_index("sp"), lax.axis_index("tp")
@@ -589,15 +589,16 @@
             psend.at[unit, h], precv.at[unit, h], p_send, p_recv.at[unit, h], there(g, z, partner)
         )
 
-    def x_copy(unit, h, j, zz):
+    def x_copy(unit, h, j, far):
         xx = lax.rem(x + j, half)
+        zz = 1 - zi if far else zi
         return remote(
             msend.at[unit, h, zz, xx], xrecv.at[unit, h, x, zz],
-            x_send, x_recv.at[unit, h, zz], there(g, z, xx * 2 + core),
-        )
-
-    def x_wait(unit, h, zz):
-        await_recv(xrecv.at[unit, h, pl.ds(0, half - 1), zz], x_recv.at[unit, h, zz])
+            x_send, x_recv.at[unit, h] if far else x_home, there(g, z, xx * 2 + core),
+        )
+
+    def x_wait(unit, h):
+        await_recv(xrecv.at[unit, h, pl.ds(0, half - 1), 0], x_recv.at[unit, h])
 
     def z_copy(unit, h):
         return remote(
@@ -638,10 +639,10 @@
             msend[unit, h] = total.astype(BF16).reshape(msend.shape[2:])
             if group > 1:
                 for j in range(1, half):
-                    x_copy(unit, h, j, 1 - zi).start()
+                    x_copy(unit, h, j, True).start()
         for h in range(parts):
             for j in range(1, half):
-                x_copy(unit, h, j, zi).start()
+                x_copy(unit, h, j, False).start()
             for zz in range(group):
                 xrecv[unit, h, x, zz] = msend[unit, h, zz, x]
 
@@ -655,7 +656,7 @@
         unit = unit_of(m)
         if group > 1:
             for h in range(parts):
-                x_wait(unit, h, 1 - zi)
+                x_wait(unit, h)
                 zsend[unit, h] = gathered(unit, h, 1 - zi).astype(BF16)
                 z_copy(unit, h).start()
 
@@ -700,12 +701,13 @@
         hand_over(units - 2)
     hand_over(units - 1)
 
+    if half > 1:
+        await_recv(xrecv.at[:, :, pl.ds(0, half - 1), 0], x_home)
     direct = out_cols % 128 == 0 and n % 128 == 0
 
     def finish(m, _):
         unit = unit_of(m)
         for h in range(parts):
-            x_wait(unit, h, zi)
             total = gathered(unit, h, zi)
             if group > 1:
                 z_copy(unit, h).wait_recv()
@@ -776,6 +778,12 @@
     vmem = pl.BlockSpec(memory_space=pltpu.VMEM)
     hbm = pl.BlockSpec(memory_space=pl.ANY)
     dma = pltpu.SemaphoreType.DMA
+    arrays = (
+        queries, memory_keys, memory_values, output_preactivation,
+        input_preactivation, forget_preactivation, extra_forget_terms,
+        head_norm_gain.reshape(1, dh), output_projection_matrix, residual,
+        feedforward_norm_gain.reshape(1, width), feedforward_up_matrix, feedforward_down_matrix,
+    )
     return pl.pallas_call(
         functools.partial(
             kernel, (grp, sp, tp, heads, blocks, rows, group, usubs, rsubs, pieces, tsubs, parts)
@@ -824,7 +832,7 @@
             dma,
             dma((sp, dsubs)),
             dma,
-            dma((sp, pieces, grp)),
+            dma((sp, pieces, max(grp - 1, 1))),
             dma,
             dma((tp,)),
             dma((2,)),
@@ -837,18 +845,16 @@
             dma,
             dma((units, parts)),
             dma,
-            dma((units, parts, group)),
+            dma((units, parts)),
+            dma,
             dma,
             dma((units, parts)),
         ],
         compiler_params=pltpu.CompilerParams(
-            collective_id=0, has_side_effects=True, vmem_limit_bytes=60 * 1024 * 1024
+            collective_id=0, has_side_effects=True, vmem_limit_bytes=44 * 1024 * 1024
         ),
     )(
-        queries, memory_keys, memory_values, output_preactivation,
-        input_preactivation, forget_preactivation, extra_forget_terms,
-        head_norm_gain.reshape(1, dh), output_projection_matrix, residual,
-        feedforward_norm_gain.reshape(1, width), feedforward_up_matrix, feedforward_down_matrix,
+        *(pltpu.with_memory_space_constraint(array, pltpu.HBM) for array in arrays)
     )
 
 

time: 113 us -> 111 us (0.982)
  no operation moved by 1% of the time
where the time goes in v5:
time: 111 us
  Pallas kernels  110 us (99%)
    pallas_call x1, Pallas kernels, shards(): pl.pallas_call(functools.partial(kernel, (grp, sp, tp, heads, blocks, row...  110 us

profile of v5, /device:TPU:17, one launch (start us, length us, event | category | flops | bytes accessed | tf_op | source)
XLA Modules:
  0.0 110.5 jit_solution(11800197644161965440)
XLA Ops:
  0.0 109.7 %shard_map.127 = bf16[128,2048]{1,0:T(8,128)(2,1)S(1)} custom-call(bf16[512,256]{1,0:T(8,128)(2,1)} %q_hbm.1, bf16[512,256]{1,0:T(8,128)(2,1)} %k_hbm.1, bf16[512,256]{1,0:T(8,128)(2,1)} %v_hbm.1, bf16[512,256]{1,0:T(8,128)(2,1)} %o_hbm.1, f32[2,512]{1,0:T(2,128)} %igate_hbm.1, f32[2,512]{1,0:T(2,128)} %fgate_hbm.1, f32[2,512]{1,0:T(2,128)} %extra_hbm.1, ...), custom_call_target="tpu_custom_call" | custom-call | tf_op jit(solution)/shard_map/pallas_call | solution.py:787
  109.7 0.8 copy.15

commit v6 on v5

--- a/solution.py
+++ b/solution.py
@@ -72,16 +72,17 @@
             src_ref=src, dst_ref=dst, send_sem=send, recv_sem=recv, device_id=where, device_id_type=MESH
         )
 
-    def nth(k):
+    def nth(k, zz=None):
+        zz = z if zz is None else zz
         power = sp & (sp - 1) == 0
         if not power:
-            return lax.rem(z + k, sp)
+            return lax.rem(zz + k, sp)
         gray_of = k
         total = 0
         bit = 1
         while bit < sp:
             mask = (gray_of // bit + gray_of // (2 * bit)) % 2
-            zbit = lax.rem(z // bit, 2)
+            zbit = lax.rem(zz // bit, 2)
             total = total + (zbit + mask - 2 * zbit * mask) * bit
             bit *= 2
         return total
@@ -136,11 +137,13 @@
         )
 
     def down_copy(zz, s):
+        final = (nth(sp - 1, zz) == z).astype(jnp.int32)
+        slot = (z * pieces + s // rsubs) * (1 - final) + (sp * pieces + s) * final
         first = lax.rem(zz, group) * part + g * (drows * rsubs) + s % rsubs * drows
         return remote(
             down_hbm.at[pl.ds(aligned(first, 16), drows), pl.ds(s // rsubs * n, n)],
             dnw.at[(z, *down_at(g, s))],
-            wd_send, wd_recv.at[z, s], there(g, zz, t),
+            wd_send, wd_recv.at[slot], there(g, zz, t),
         )
 
     def up_pass(o, s, j):
@@ -162,12 +165,32 @@
             for j in range(1, grp):
                 up_pass(o, s, j).start()
 
+    def relay_parts(o, c):
+        for s in of_piece(c):
+            await_recv(dnw.at[(o, *down_at(g, s))], wd_recv.at[sp * pieces + s])
+            for j in range(1, grp):
+                down_pass(o, s, j).start()
+
+    def relay_whole(o, c):
+        at = dnw.at[o, pl.ds(aligned(g * (drows * rsubs), 16), drows * rsubs), pl.ds(c * n, n)]
+        await_recv(at, wd_recv.at[o * pieces + c])
+        for j in range(1, grp):
+            where = there(lax.rem(g + j, grp), z, t)
+            remote(at, at, dy_send, dy_recv.at[o, c, grp - j - 1], where).start()
+
     def relay_down(k, c):
         o = nth(k)
-        for s in of_piece(c):
-            await_recv(dnw.at[(o, *down_at(g, s))], wd_recv.at[o, s])
-            for j in range(1, grp):
-                down_pass(o, s, j).start()
+        if isinstance(k, int):
+            (relay_parts if k == sp - 1 else relay_whole)(o, c)
+            return
+
+        @pl.when(k == sp - 1)
+        def _():
+            relay_parts(o, c)
+
+        @pl.when(k < sp - 1)
+        def _():
+            relay_whole(o, c)
 
     def finish_down(k, c):
         o = nth(k)
@@ -764,7 +787,7 @@
     part = hidden // group
     usubs = 2 if up_rows % (32 * grp) == 0 else 1
     pieces = 2 if out_cols % 256 == 0 else 1
-    rsubs = 4 if part % (64 * grp) == 0 else 1
+    rsubs = 8 if part % (128 * grp) == 0 else 1
     dsubs = rsubs * pieces
     tsubs = 4 if rows % 64 == 0 else 1
     half = tp // 2
@@ -830,7 +853,7 @@
             dma,
             dma,
             dma,
-            dma((sp, dsubs)),
+            dma((sp * pieces + dsubs,)),
             dma,
             dma((sp, pieces, max(grp - 1, 1))),
             dma,

time: 111 us -> 110 us (level)
  no operation moved by 1% of the time
where the time goes in v6:
time: 110 us
  Pallas kernels  109 us (99%)
    pallas_call x1, Pallas kernels, shards(): pl.pallas_call(functools.partial(kernel, (grp, sp, tp, heads, blocks, row...  109 us

profile of v6, /device:TPU:17, one launch (start us, length us, event | category | flops | bytes accessed | tf_op | source)
XLA Modules:
  0.0 109.7 jit_solution(17742378141880545750)
XLA Ops:
  0.0 108.9 %shard_map.127 = bf16[128,2048]{1,0:T(8,128)(2,1)S(1)} custom-call(bf16[512,256]{1,0:T(8,128)(2,1)} %q_hbm.1, bf16[512,256]{1,0:T(8,128)(2,1)} %k_hbm.1, bf16[512,256]{1,0:T(8,128)(2,1)} %v_hbm.1, bf16[512,256]{1,0:T(8,128)(2,1)} %o_hbm.1, f32[2,512]{1,0:T(2,128)} %igate_hbm.1, f32[2,512]{1,0:T(2,128)} %fgate_hbm.1, f32[2,512]{1,0:T(2,128)} %extra_hbm.1, ...), custom_call_target="tpu_custom_call" | custom-call | tf_op jit(solution)/shard_map/pallas_call | solution.py:810
  109.0 0.8 copy.15
